TPU v7x, 32 devices: a whole 2x2x4 slice. The times are simulated.
32 devices in a mesh: grp: 2 (over y), tp: 4 (over z), dp: 4 (over x, core).
Axes of the slice: x: 2, y: 2, z: 4, core: 2. Of those that a mesh axis runs over, the one named last changes fastest.
Arguments:
- tokens: bfloat16 [128, 8, 2048], P('grp', None, 'dp'), parts along dimension 0, may hold values from -64 to 64
- live_counts: int32 [128], P(('grp', 'dp')), parts along dimension 0, may hold values from 1 to 8, 256 in all
- norm_gain: float32 [2, 2048], P(None, 'dp'), may hold values from 0.1 to 1.9
- w_branch: bfloat16 [2, 2048, 4096], P(None, 'dp', 'tp'), may hold values from -0.125 to 0.125
- w_silu_gate: bfloat16 [2, 2048, 4096], P(None, 'dp', 'tp'), may hold values from -0.125 to 0.125
- conv_weight: float32 [2, 4, 4096], P(None, None, 'tp'), may hold values from -3 to 3
- w_query: bfloat16 [2, 16, 256, 256], P(None, 'tp'), may hold values from -0.375 to 0.375
- w_key: bfloat16 [2, 16, 256, 256], P(None, 'tp'), may hold values from -0.375 to 0.375
- w_value: bfloat16 [2, 16, 256, 256], P(None, 'tp'), may hold values from -0.375 to 0.375
- w_input_gate: bfloat16 [2, 16, 768], P(None, 'tp'), may hold values from -0.21875 to 0.21875
- w_forget_gate: bfloat16 [2, 16, 768], P(None, 'tp'), may hold values from -0.21875 to 0.21875
- bias_input: float32 [2, 16], P(None, 'tp'), may hold values from -2 to 2
- bias_forget: float32 [2, 16], P(None, 'tp'), may hold values from -1 to 5
- out_gain: float32 [2, 16, 256], P(None, 'tp'), may hold values from 0.25 to 4
- skip_gain: float32 [2, 4096], P(None, 'tp'), may hold values from 0.25 to 4
- w_out: bfloat16 [2, 4096, 2048], P(None, 'tp', 'dp'), may hold values from -0.09375 to 0.09375
- conv_state: bfloat16 [2, 128, 3, 4096], P(None, ('grp', 'dp'), None, 'tp'), parts along dimension 1, may hold values from -6 to 6
- memory: float32 [2, 128, 16, 256, 256], P(None, ('grp', 'dp'), 'tp'), parts along dimension 1, may hold values from -0.375 to 0.375
- max_state: float32 [2, 128, 16], P(None, ('grp', 'dp'), 'tp'), parts along dimension 1, may hold values from -4 to 4
Outputs:
- out_tokens: bfloat16 [128, 8, 2048], P('grp', None, 'dp'), parts along dimension 0
- new_conv_state: bfloat16 [2, 128, 3, 4096], P(None, ('grp', 'dp'), None, 'tp'), parts along dimension 1
- new_memory: float32 [2, 128, 16, 256, 256], P(None, ('grp', 'dp'), 'tp'), parts along dimension 1
- new_max: float32 [2, 128, 16], P(None, ('grp', 'dp'), 'tp'), parts along dimension 1
There are 2 independent parts, one for each index of `grp`. A program takes and returns all parts, laid end to end along the dimension named above; an argument that names none is the same for every part. Nothing has to cross between parts.
Inputs may be any that keep to these rules, and one draw needn't show every extreme that they name: `live_counts`: each sequence has at least one live slot; within each part (each independent copy of the problem) the 64 counts sum to 256, so the whole array sums to that times the number of parts; in each part some sequence uses all 8 slots.
All inputs are finite; a program needn't handle non-finite values. No bound on the sum of `live_counts` on one device may be relied on, other than what follows from the above.
Results may differ from a plain program's by a relative error of at most 0.035.
Values may be sent and summed in bfloat16 or wider, within the bound.
A program may use at most 192 MiB of HBM per device.

v0:
```python
import jax
import jax.numpy as jnp
from jax import lax
from jax.sharding import PartitionSpec as P

D = 2048
HEAD_DIM = 256
CONV = 4
LAYERS = 2


epsilon = 1e-06
very_negative = -1e30


def recurrent_cell(
    branch,
    silu_gate,
    live_counts,
    conv_weight,
    w_query,
    w_key,
    w_value,
    w_input_gate,
    w_forget_gate,
    bias_input,
    bias_forget,
    out_gain,
    skip_gain,
    conv_state,
    memory,
    max_state,
):
    local_batch = branch.shape[0]
    steps = branch.shape[1]
    local_width = branch.shape[2]
    local_heads = w_query.shape[0]
    padded = jnp.concatenate([conv_state, branch], axis=1)
    conv_sum = jnp.zeros((local_batch, steps, local_width), jnp.float32)
    for offset in range(CONV):
        conv_sum = (
            conv_sum + padded[:, offset : offset + steps].astype(jnp.float32) * conv_weight[offset]
        )
    convolved = jax.nn.silu(conv_sum).astype(jnp.bfloat16)
    picks = live_counts[:, None] + jnp.arange(CONV - 1, dtype=jnp.int32)[None, :]
    new_conv = jnp.take_along_axis(padded, picks[:, :, None], axis=1)
    conv_heads = convolved.reshape(local_batch, steps, local_heads, HEAD_DIM)
    branch_heads = branch.reshape(local_batch, steps, local_heads, HEAD_DIM)
    queries = jnp.einsum(
        "blhd,hde->blhe", conv_heads, w_query, preferred_element_type=jnp.float32
    ).astype(jnp.bfloat16)
    key_rows = jnp.einsum(
        "blhd,hde->blhe", conv_heads, w_key, preferred_element_type=jnp.float32
    ).astype(jnp.bfloat16)
    value_rows = jnp.einsum(
        "blhd,hde->blhe", branch_heads, w_value, preferred_element_type=jnp.float32
    ).astype(jnp.bfloat16)
    joined = jnp.concatenate([queries, key_rows, value_rows], axis=-1)
    input_log = (
        jnp.einsum("blhc,hc->blh", joined, w_input_gate, preferred_element_type=jnp.float32)
        + bias_input
    )
    forget_pre = (
        jnp.einsum("blhc,hc->blh", joined, w_forget_gate, preferred_element_type=jnp.float32)
        + bias_forget
    )
    forget_log = jax.nn.log_sigmoid(forget_pre)
    positions = jnp.arange(steps, dtype=jnp.int32)
    live = positions[None, :] < live_counts[:, None]
    input_log = jnp.transpose(jnp.where(live[:, :, None], input_log, very_negative), (0, 2, 1))
    forget_log = jnp.transpose(jnp.where(live[:, :, None], forget_log, 0.0), (0, 2, 1))
    query_heads = jnp.transpose(queries.astype(jnp.float32), (0, 2, 1, 3))
    key_heads = jnp.transpose(key_rows.astype(jnp.float32), (0, 2, 1, 3)) * HEAD_DIM ** (-0.5)
    value_heads = jnp.transpose(value_rows.astype(jnp.float32), (0, 2, 1, 3))
    cumulative = jnp.cumsum(forget_log, axis=-1)
    log_weights = cumulative[..., :, None] - cumulative[..., None, :] + input_log[..., None, :]
    causal = positions[:, None] >= positions[None, :]
    log_weights = jnp.where(causal, log_weights, very_negative)
    carried = cumulative + max_state[..., None]
    stabilizer = jnp.maximum(jnp.max(log_weights, axis=-1), carried)
    weights = jnp.exp(log_weights - stabilizer[..., None])
    carried_scale = jnp.exp(carried - stabilizer)
    scores = jnp.einsum("bhtd,bhsd->bhts", query_heads, key_heads) * weights
    numerator = jnp.einsum("bhts,bhse->bhte", scores, value_heads)
    numerator = numerator + carried_scale[..., None] * jnp.einsum(
        "bhtd,bhde->bhte", query_heads, memory
    )
    centered = numerator - jnp.mean(numerator, axis=-1, keepdims=True)
    normalized = centered * lax.rsqrt(
        jnp.mean(centered * centered, axis=-1, keepdims=True) + epsilon
    )
    normalized = normalized * out_gain[None, :, None, :]
    readout = jnp.transpose(normalized, (0, 2, 1, 3)).reshape(local_batch, steps, local_width)
    new_max = stabilizer[..., -1]
    decay = jnp.exp(cumulative[..., -1] + max_state - new_max)
    update_weight = jnp.exp(cumulative[..., -1:] - cumulative + input_log - new_max[..., None])
    new_memory = decay[..., None, None] * memory + jnp.einsum(
        "bhs,bhsd,bhse->bhde", update_weight, key_heads, value_heads
    )
    mixed = (readout + skip_gain * convolved.astype(jnp.float32)) * jax.nn.silu(
        silu_gate.astype(jnp.float32)
    )
    mixed = jnp.where(live[:, :, None], mixed, 0.0).astype(jnp.bfloat16)
    return (mixed, new_conv, new_memory, new_max)


def layer_step(
    tokens,
    live_counts,
    gain,
    w_branch,
    w_silu_gate,
    conv_weight,
    w_query,
    w_key,
    w_value,
    w_input_gate,
    w_forget_gate,
    bias_input,
    bias_forget,
    out_gain,
    skip_gain,
    w_out,
    conv_state,
    memory,
    max_state,
):
    all_batch = tokens.shape[0]
    steps = tokens.shape[1]
    local_features = tokens.shape[2]
    local_width = w_branch.shape[1]
    local_batch = live_counts.shape[0]
    floats = tokens.astype(jnp.float32)
    partial_squares = jnp.sum(floats * floats, axis=-1)
    total_squares = lax.psum(partial_squares, "dp")
    normed = (floats * lax.rsqrt(total_squares / D + epsilon)[..., None] * gain).astype(
        jnp.bfloat16
    )
    rows = normed.reshape(local_batch * lax.axis_size("dp") * steps, local_features)
    first = jnp.dot(rows, w_branch, preferred_element_type=jnp.float32)
    second = jnp.dot(rows, w_silu_gate, preferred_element_type=jnp.float32)
    summed = lax.psum_scatter(
        jnp.stack([first, second], axis=1)
        .reshape(local_batch * lax.axis_size("dp"), steps, 2, local_width)
        .astype(jnp.bfloat16),
        "dp",
        scatter_dimension=0,
        tiled=True,
    ).astype(jnp.float32)
    branch = summed[:, :, 0].astype(jnp.bfloat16)
    silu_gate = summed[:, :, 1].astype(jnp.bfloat16)
    mixed, new_conv, new_memory, new_max = recurrent_cell(
        branch,
        silu_gate,
        live_counts,
        conv_weight,
        w_query,
        w_key,
        w_value,
        w_input_gate,
        w_forget_gate,
        bias_input,
        bias_forget,
        out_gain,
        skip_gain,
        conv_state,
        memory,
        max_state,
    )
    piece = lax.all_gather(mixed, "dp", axis=0, tiled=True)
    flat = piece.reshape(piece.shape[0] * steps, local_width)
    product = jnp.dot(flat, w_out, preferred_element_type=jnp.float32)
    terms = product.reshape(piece.shape[0], steps, local_features)
    flat_terms = terms.reshape(all_batch * steps, local_features)
    share = lax.psum_scatter(
        flat_terms.astype(jnp.bfloat16), "tp", scatter_dimension=0, tiled=True
    ).astype(jnp.float32)
    share_rows = share.shape[0]
    residual_rows = lax.dynamic_slice_in_dim(
        floats.reshape(all_batch * steps, local_features),
        lax.axis_index("tp") * share_rows,
        share_rows,
        0,
    )
    new_share = (residual_rows + share.astype(jnp.bfloat16).astype(jnp.float32)).astype(
        jnp.bfloat16
    )
    result = lax.all_gather(new_share, "tp", axis=0, tiled=True).reshape(
        all_batch, steps, local_features
    )
    return (result, new_conv, new_memory, new_max)


def per_device(
    tokens,
    live_counts,
    norm_gain,
    w_branch,
    w_silu_gate,
    conv_weight,
    w_query,
    w_key,
    w_value,
    w_input_gate,
    w_forget_gate,
    bias_input,
    bias_forget,
    out_gain,
    skip_gain,
    w_out,
    conv_state,
    memory,
    max_state,
):
    stream = tokens
    conv_list = []
    memory_list = []
    max_list = []
    for which_layer in range(LAYERS):
        stream, new_conv, new_memory, new_max = layer_step(
            stream,
            live_counts,
            norm_gain[which_layer],
            w_branch[which_layer],
            w_silu_gate[which_layer],
            conv_weight[which_layer],
            w_query[which_layer],
            w_key[which_layer],
            w_value[which_layer],
            w_input_gate[which_layer],
            w_forget_gate[which_layer],
            bias_input[which_layer],
            bias_forget[which_layer],
            out_gain[which_layer],
            skip_gain[which_layer],
            w_out[which_layer],
            conv_state[which_layer],
            memory[which_layer],
            max_state[which_layer],
        )
        conv_list.append(new_conv)
        memory_list.append(new_memory)
        max_list.append(new_max)
    return (stream, jnp.stack(conv_list), jnp.stack(memory_list), jnp.stack(max_list))


def solution(mesh):
    in_specs = (
        P("grp", None, "dp"),
        P(("grp", "dp")),
        P(None, "dp"),
        P(None, "dp", "tp"),
        P(None, "dp", "tp"),
        P(None, None, "tp"),
        P(None, "tp", None, None),
        P(None, "tp", None, None),
        P(None, "tp", None, None),
        P(None, "tp", None),
        P(None, "tp", None),
        P(None, "tp"),
        P(None, "tp"),
        P(None, "tp", None),
        P(None, "tp"),
        P(None, "tp", "dp"),
        P(None, ("grp", "dp"), None, "tp"),
        P(None, ("grp", "dp"), "tp", None, None),
        P(None, ("grp", "dp"), "tp"),
    )
    out_specs = (
        P("grp", None, "dp"),
        P(None, ("grp", "dp"), None, "tp"),
        P(None, ("grp", "dp"), "tp", None, None),
        P(None, ("grp", "dp"), "tp"),
    )
    return jax.shard_map(
        per_device, mesh=mesh, in_specs=in_specs, out_specs=out_specs, check_vma=False
    )
```

profile of v0, /device:TPU:0, one launch (start us, length us, event | category | flops | bytes accessed | tf_op | source)
XLA Modules:
  0.0 297.1 jit_solution(8914190688373300822)
XLA Ops:
  7.2 1.4 fusion.162
  9.9 12.9 %psum.14 = f32[64,8]{1,0:T(8,128)S(1)} all-reduce(f32[64,8]{1,0:T(8,128)S(1)} %fusion.16), channel_id=1, replica_groups=mesh['grp'=2,'tp'=4,'dp'=4] {'dp'}, use_global_device_ids=true, to_apply=%region_1.0 | all-reduce | flops 512 | bytes 4096 | tf_op jit(solution)/shard_map/psum | solution.py:135
  22.8 2.1 fusion.11
  26.2 2.5 copy.279
  34.3 26.1 %reduce-scatter.15.cloned.1.call-done = bf16[16,16384]{1,0:T(8,128)(2,1)} async-done(((bf16[64,16384]{1,0:T(8,128)(2,1)}), bf16[16,16384]{1,0:T(8,128)(2,1)}) %reduce-scatter.15.cloned.1.call-update) | async-done | bytes 524304
  60.5 1.4 copy.280
  65.6 1.8 fusion.76
  67.4 1.8 fusion.77
  69.4 2.8 reduce_window_sum.17
  75.2 7.0 %fusion.4 = f32[16,4,8,256]{3,2,1,0:T(8,128)S(1)} fusion(f32[2,16,4,256,256]{4,3,2,1,0:T(8,128)} %param.38, bf16[4,16,8,256]{3,2,1,0:T(8,128)(2,1)S(1)} %convolution_convert_fusion.11), kind=kOutput, calls=%fused_computation.9 | convolution fusion | flops 67108864 | bytes 9175040 | tf_op jit(solution)/shard_map/bhtd,bhde->bhte/dot_general | solution.py:85
  85.8 16.8 %all-gather.3.cloned.1.call-done = bf16[64,8,1024]{2,1,0:T(8,128)(2,1)} async-done(((bf16[16,8,1024]{2,1,0:T(8,128)(2,1)}), bf16[64,8,1024]{2,1,0:T(8,128)(2,1)}) %all-gather.3.cloned.1.call-update) | async-done | bytes 1048592 | tf_op jit(solution)/shard_map/all_gather | solution.py:170
  102.6 3.0 %convolution_convert_fusion.5 = bf16[512,512]{1,0:T(8,128)(2,1)} fusion(bf16[64,8,1024]{2,1,0:T(8,128)(2,1)} %all-gather.3.cloned.1.call-done, bf16[2,1024,512]{2,1,0:T(8,128)(2,1)} %param.36), kind=kOutput, calls=%fused_computation.29 | convolution fusion | flops 537133056 | bytes 2621440 | tf_op jit(solution)/shard_map/dot_general | solution.py:172
  105.8 21.8 %reduce-scatter.11.cloned.1.call-done = bf16[128,512]{1,0:T(8,128)(2,1)} async-done(((bf16[512,512]{1,0:T(8,128)(2,1)}), bf16[128,512]{1,0:T(8,128)(2,1)}) %reduce-scatter.11.cloned.1.call-update) | async-done | bytes 131088 | tf_op jit(solution)/shard_map/reduce_scatter | solution.py:175
  128.6 15.6 %all_gather.13 = bf16[512,512]{1,0:T(8,128)(2,1)S(1)} all-gather(bf16[128,512]{1,0:T(8,128)(2,1)S(1)} %add_convert_fusion.1), channel_id=1, replica_groups=mesh['grp'=2,'tp'=4,'dp'=4] {'tp'}, dimensions={0}, use_global_device_ids=true | all-gather | bytes 655360 | tf_op jit(solution)/shard_map/all_gather | solution.py:188
  144.4 10.3 %psum.15 = f32[64,8]{1,0:T(8,128)S(1)} all-reduce(f32[64,8]{1,0:T(8,128)S(1)} %reduce_sum.60), channel_id=1, replica_groups=mesh['grp'=2,'tp'=4,'dp'=4] {'dp'}, use_global_device_ids=true, to_apply=%region_9.10 | all-reduce | flops 512 | bytes 4096 | tf_op jit(solution)/shard_map/psum | solution.py:135
  154.8 2.0 fusion.13
  156.8 2.0 fusion.12
  159.2 2.5 copy.281
  163.5 28.2 %reduce-scatter.17.cloned.1.call-done = bf16[16,16384]{1,0:T(8,128)(2,1)} async-done(((bf16[64,16384]{1,0:T(8,128)(2,1)}), bf16[16,16384]{1,0:T(8,128)(2,1)}) %reduce-scatter.17.cloned.1.call-update) | async-done | bytes 524304
  196.8 1.4 convolution_convert_fusion.7
  198.2 1.5 convolution_convert_fusion.6
  199.8 1.8 fusion.74
  201.6 1.8 fusion.75
  203.6 2.8 reduce_window_sum.18
  207.1 7.1 %fusion = f32[16,4,8,256]{3,2,1,0:T(8,128)S(1)} fusion(f32[2,16,4,256,256]{4,3,2,1,0:T(8,128)} %param.38, bf16[4,16,8,256]{3,2,1,0:T(8,128)(2,1)} %copy-done.1), kind=kOutput, calls=%fused_computation.4 | convolution fusion | flops 67108864 | bytes 9175040 | tf_op jit(solution)/shard_map/bhtd,bhde->bhte/dot_general | solution.py:85
  218.7 1.7 bitcast_multiply_fusion.3
  220.4 1.5 fusion.109
  225.1 10.8 %fusion.3 = f32[1,16,4,256,256]{4,3,2,1,0:T(8,128)} fusion(f32[2,16,4,256,256]{4,3,2,1,0:T(8,128)} %param.38, f32[16,4]{1,0:T(8,128)S(1)} %copy.242, bf16[16,4,8,256]{3,2,0,1:T(8,128)(2,1)S(1)} %get-tuple-element.27, bf16[4,16,8,256]{3,2,1,0:T(8,128)(2,1)S(1)} %copy-done.9), kind=kOutput, calls=%fused_computation.7 | convolution fusion | flops 75497472 | bytes 34078976 | tf_op jit(solution)/shard_map/bhs,bhsd,bhse->bhde/dot_general | solution.py:97
  236.0 10.8 %fusion.7 = f32[1,16,4,256,256]{4,3,2,1,0:T(8,128)} fusion(f32[2,16,4,256,256]{4,3,2,1,0:T(8,128)} %param.38, f32[16,4]{1,0:T(8,128)S(1)} %copy.234, bf16[16,4,8,256]{3,2,0,1:T(8,128)(2,1)S(1)} %get-tuple-element.25, bf16[4,16,8,256]{3,2,1,0:T(8,128)(2,1)S(1)} %copy-done.7), kind=kOutput, calls=%fused_computation.12 | convolution fusion | flops 75497472 | bytes 34078976 | tf_op jit(solution)/shard_map/bhs,bhsd,bhse->bhde/dot_general | solution.py:97
  246.8 3.0 %convolution_convert_fusion.4 = bf16[512,512]{1,0:T(8,128)(2,1)} fusion(bf16[64,8,1024]{2,1,0:T(8,128)(2,1)} %all-gather.5.cloned.1.call-done, bf16[2,1024,512]{2,1,0:T(8,128)(2,1)} %param.36), kind=kOutput, calls=%fused_computation.28 | convolution fusion | flops 537133056 | bytes 2621440 | tf_op jit(solution)/shard_map/dot_general | solution.py:172
  249.9 23.1 %pad_maximum_fusion = f32[2,16,4,256,256]{4,3,2,1,0:T(8,128)} fusion(f32[1,16,4,256,256]{4,3,2,1,0:T(8,128)} %fusion.3, f32[1,16,4,256,256]{4,3,2,1,0:T(8,128)} %fusion.7), kind=kLoop, calls=%fused_computation.2 | loop fusion | flops 8388608 | bytes 67108864 | tf_op jit(solution)/shard_map/stack | solution.py:244
  273.9 15.6 %all_gather.15 = bf16[512,512]{1,0:T(8,128)(2,1)S(1)} all-gather(bf16[128,512]{1,0:T(8,128)(2,1)S(1)} %add_convert_fusion), channel_id=1, replica_groups=mesh['grp'=2,'tp'=4,'dp'=4] {'tp'}, dimensions={0}, use_global_device_ids=true | all-gather | bytes 655360 | tf_op jit(solution)/shard_map/all_gather | solution.py:188
  (216 shorter events, 37.0 us)
Async XLA Ops:
  7.2 17.8 %copy-start = (bf16[64,8,512]{2,1,0:T(8,128)(2,1)S(1)}, bf16[64,8,512]{2,1,0:T(8,128)(2,1)}, u32[]{:S(2)}) copy-start(bf16[64,8,512]{2,1,0:T(8,128)(2,1)} %param.21) | copy-start | bytes 1572868
  7.2 17.8 %copy-start.47 = (bf16[2,512,1024]{2,1,0:T(8,128)(2,1)S(1)}, bf16[2,512,1024]{2,1,0:T(8,128)(2,1)}, u32[]{:S(2)}) copy-start(bf16[2,512,1024]{2,1,0:T(8,128)(2,1)} %param.24) | copy-start | bytes 6291460
  7.2 53.3 %reduce-scatter.15.cloned.1.call-start = ((), (), s32[]{:S(2)}) async-start(), calls=%async_computation.8 | async-start | bytes 2621440
  28.7 3.7 %copy-start.26 = (bf16[2,4,768]{2,1,0:T(4,128)(2,1)S(1)}, bf16[2,4,768]{2,1,0:T(4,128)(2,1)}, u32[]{:S(2)}) copy-start(bf16[2,4,768]{2,1,0:T(4,128)(2,1)} %param.30) | copy-start | bytes 36868
  28.7 4.3 %copy-start.27 = (bf16[2,4,768]{2,1,0:T(4,128)(2,1)S(1)}, bf16[2,4,768]{2,1,0:T(4,128)(2,1)}, u32[]{:S(2)}) copy-start(bf16[2,4,768]{2,1,0:T(4,128)(2,1)} %param.31) | copy-start | bytes 36868
  28.8 4.9 %copy-start.14 = (f32[2,4,1024]{2,1,0:T(4,128)S(1)}, f32[2,4,1024]{2,1,0:T(4,128)}, u32[]{:S(2)}) copy-start(f32[2,4,1024]{2,1,0:T(4,128)} %param.26) | copy-start | bytes 98308
  28.8 5.5 %copy-start.11 = (bf16[2,16,3,1024]{3,1,2,0:T(8,128)(2,1)S(1)}, bf16[2,16,3,1024]{3,1,2,0:T(8,128)(2,1)}, u32[]{:S(2)}) copy-start(bf16[2,16,3,1024]{3,1,2,0:T(8,128)(2,1)} %param.37) | copy-start | bytes 589828
  28.8 73.8 %all-gather.3.cloned.1.call-start = ((), (), s32[]{:S(2)}) async-start(), calls=%async_computation.4 | async-start | bytes 1310720 | tf_op jit(solution)/shard_map/all_gather | solution.py:170
  29.4 32.5 %copy-start.28 = (pred[16,8]{0,1:T(8,128)(4,1)}, pred[16,8]{0,1:T(8,128)(4,1)S(1)}, u32[]{:S(2)}) copy-start(pred[16,8]{0,1:T(8,128)(4,1)S(1)} %iota_compare_fusion.1) | copy-start | bytes 388
  30.1 42.2 %copy-start.39 = (pred[8,8]{1,0:T(8,128)(4,1)}, pred[8,8]{1,0:T(8,128)(4,1)S(1)}, u32[]{:S(2)}) copy-start(pred[8,8]{1,0:T(8,128)(4,1)S(1)} %iota_compare_fusion) | copy-start | bytes 196
  30.7 41.6 %copy-start.38 = (f32[4]{0:T(128)}, f32[4]{0:T(128)S(1)}, u32[]{:S(2)}) copy-start(f32[4]{0:T(128)S(1)} %get-tuple-element.66) | copy-start | bytes 52
  65.6 16.6 %copy-start.6 = (bf16[4,16,8,256]{3,2,1,0:T(8,128)(2,1)}, bf16[4,16,8,256]{3,2,1,0:T(8,128)(2,1)S(1)}, u32[]{:S(2)}) copy-start(bf16[4,16,8,256]{3,2,1,0:T(8,128)(2,1)S(1)} %convolution_convert_fusion.9) | copy-start | bytes 786436
  73.5 8.7 %copy-start.15 = (f32[16,4,1]{0,1,2:T(4,128)}, f32[16,4,1]{0,1,2:T(4,128)S(1)}, u32[]{:S(2)}) copy-start(f32[16,4,1]{0,1,2:T(4,128)S(1)} %copy.232) | copy-start | bytes 772
  75.2 7.0 %copy-start.13 = (f32[16,4,8]{2,1,0:T(4,128)S(1)}, f32[16,4,8]{2,1,0:T(4,128)}, u32[]{:S(2)}) copy-start(f32[16,4,8]{2,1,0:T(4,128)} %copy-done.12) | copy-start | bytes 6148
  85.7 41.9 %reduce-scatter.11.cloned.1.call-start = ((), (), s32[]{:S(2)}) async-start(), calls=%async_computation.5 | async-start | bytes 655360 | tf_op jit(solution)/shard_map/reduce_scatter | solution.py:175
  105.6 49.1 %copy-start.42 = (f32[1,512]{1,0:T(1,128)S(1)}, f32[1,512]{1,0:T(1,128)}, u32[]{:S(2)}) copy-start(f32[1,512]{1,0:T(1,128)} %get-tuple-element.60) | copy-start | bytes 6148
  105.6 86.0 %reduce-scatter.17.cloned.1.call-start = ((), (), s32[]{:S(2)}) async-start(), calls=%async_computation.9 | async-start | bytes 2621440
  161.7 85.1 %all-gather.5.cloned.1.call-start = ((), (), s32[]{:S(2)}) async-start(), calls=%async_computation.6 | async-start | bytes 1310720 | tf_op jit(solution)/shard_map/all_gather | solution.py:170
  191.6 3.2 %copy-start.20 = (f32[1,1,1024]{2,1,0:T(1,128)S(1)}, f32[1,1,1024]{2,1,0:T(1,128)}, u32[]{:S(2)}) copy-start(f32[1,1,1024]{2,1,0:T(1,128)} %get-tuple-element.44) | copy-start | bytes 12292
  195.1 4.6 %copy-start.35 = (bf16[4,768,1,1]{1,0,2,3:T(4,128)(2,1)S(1)}, bf16[4,768,1,1]{1,0,2,3:T(4,128)(2,1)}, u32[]{:S(2)}) copy-start(bf16[4,768,1,1]{1,0,2,3:T(4,128)(2,1)} %get-tuple-element.49) | copy-start | bytes 18436
  196.7 4.8 %copy-start.1 = (bf16[4,16,8,256]{3,2,1,0:T(8,128)(2,1)}, bf16[4,16,8,256]{3,2,1,0:T(8,128)(2,1)S(1)}, u32[]{:S(2)}) copy-start(bf16[4,16,8,256]{3,2,1,0:T(8,128)(2,1)S(1)} %convolution_convert_fusion.8) | copy-start | bytes 786436
  198.2 5.2 %copy-start.4 = (bf16[4,16,8,256]{3,2,1,0:T(8,128)(2,1)}, bf16[4,16,8,256]{3,2,1,0:T(8,128)(2,1)S(1)}, u32[]{:S(2)}) copy-start(bf16[4,16,8,256]{3,2,1,0:T(8,128)(2,1)S(1)} %convolution_convert_fusion.7) | copy-start | bytes 786436
  198.2 3.4 %copy-start.36 = (bf16[4,768,1,1]{1,0,2,3:T(4,128)(2,1)S(1)}, bf16[4,768,1,1]{1,0,2,3:T(4,128)(2,1)}, u32[]{:S(2)}) copy-start(bf16[4,768,1,1]{1,0,2,3:T(4,128)(2,1)} %get-tuple-element.47) | copy-start | bytes 18436
  199.7 3.7 %copy-start.8 = (bf16[4,16,8,256]{3,2,1,0:T(8,128)(2,1)}, bf16[4,16,8,256]{3,2,1,0:T(8,128)(2,1)S(1)}, u32[]{:S(2)}) copy-start(bf16[4,16,8,256]{3,2,1,0:T(8,128)(2,1)S(1)} %convolution_convert_fusion.6) | copy-start | bytes 786436
  199.7 3.7 %copy-start.41 = (f32[4]{0:T(128)S(1)}, f32[4]{0:T(128)}, u32[]{:S(2)}) copy-start(f32[4]{0:T(128)} %get-tuple-element.63) | copy-start | bytes 52
  199.7 6.7 %copy-start.37 = (f32[4]{0:T(128)S(1)}, f32[4]{0:T(128)}, u32[]{:S(2)}) copy-start(f32[4]{0:T(128)} %get-tuple-element.65) | copy-start | bytes 52
  199.8 6.7 %copy-start.40 = (pred[8,8]{1,0:T(8,128)(4,1)S(1)}, pred[8,8]{1,0:T(8,128)(4,1)}, u32[]{:S(2)}) copy-start(pred[8,8]{1,0:T(8,128)(4,1)} %copy-done.39) | copy-start | bytes 196
  214.1 4.1 %copy-start.16 = (f32[16,4,1]{0,1,2:T(4,128)S(1)}, f32[16,4,1]{0,1,2:T(4,128)}, u32[]{:S(2)}) copy-start(f32[16,4,1]{0,1,2:T(4,128)} %copy-done.15) | copy-start | bytes 772
  214.2 4.1 %copy-start.25 = (f32[2,16,4]{1,2,0:T(4,128)S(1)}, f32[2,16,4]{1,2,0:T(4,128)}, u32[]{:S(2)}) copy-start(f32[2,16,4]{1,2,0:T(4,128)} %param.39) | copy-start | bytes 1540
  215.4 5.0 %copy-start.2 = (bf16[4,16,8,256]{3,2,1,0:T(8,128)(2,1)S(1)}, bf16[4,16,8,256]{3,2,1,0:T(8,128)(2,1)}, u32[]{:S(2)}) copy-start(bf16[4,16,8,256]{3,2,1,0:T(8,128)(2,1)} %copy-done.1) | copy-start | bytes 786436
  224.3 48.7 %reduce-scatter.13.cloned.1.call-start = ((), (), s32[]{:S(2)}) async-start(), calls=%async_computation.7 | async-start | bytes 655360 | tf_op jit(solution)/shard_map/reduce_scatter | solution.py:175
  225.1 10.9 %copy-start.7 = (bf16[4,16,8,256]{3,2,1,0:T(8,128)(2,1)S(1)}, bf16[4,16,8,256]{3,2,1,0:T(8,128)(2,1)}, u32[]{:S(2)}) copy-start(bf16[4,16,8,256]{3,2,1,0:T(8,128)(2,1)} %copy-done.6) | copy-start | bytes 786436
  (24 other events, 44.8 us)
Sparse Core Ops, SparseCore 0:
  28.9 31.4 reduce-scatter.14
  85.8 16.6 all-gather.2
  105.8 21.8 reduce-scatter.10
  161.9 29.7 reduce-scatter.16
  224.4 16.7 all-gather.4
  250.0 21.9 reduce-scatter.12
where the time goes:
time: 298 us; the launch traced here: 297 us
  waiting for transfers between devices  93 us (31%)
  matrix products  65.3 us (22%)
  blocking collectives  54.3 us (18%)
  other arithmetic  41.4 us (14%)
  local copies, waits for them, and re-layouts  27.7 us (9%)
  between operations  15 us (5%)
    unnamed x8, waiting for transfers between devices  54.4 us
    all_gather x2, blocking collectives, layer_step(): lax.all_gather(new_share, 'tp', axis=0, tiled=True)  31.1 us
    psum x2, blocking collectives, layer_step(): total_squares = lax.psum(partial_squares, 'dp')  23.2 us
    another operation x1, other arithmetic, per_device(): jnp.stack(memory_list)  23.1 us
    reduce_scatter x2, waiting for transfers between devices, layer_step(): lax.psum_scatter(flat_terms.astype(jnp.bfloat16), 'tp', scatter_dimension...  21.8 us
    dot_general x2, matrix products, recurrent_cell(): jnp.einsum('bhs,bhsd,bhse->bhde', update_weight, key_heads, value_heads)  21.7 us
    all_gather x2, waiting for transfers between devices, layer_step(): piece = lax.all_gather(mixed, 'dp', axis=0, tiled=True)  16.8 us
    dot_general x2, matrix products, recurrent_cell(): jnp.einsum('bhtd,bhde->bhte', query_heads, memory)  14 us
  transfers between devices with their start and end apart: 6, of which 4 were waited for; matrix products, arithmetic and copies ran while one was open for 17% of the time, Pallas kernels for 0%

commit v1 on v0

v1 whole, which is shorter than its diff:
```python
import functools

import jax
import jax.numpy as jnp
from jax import lax
from jax.experimental import pallas as pl
from jax.experimental.pallas import tpu as pltpu
from jax.sharding import PartitionSpec as P

HEAD_DIM = 256
CONV = 4
LAYERS = 2
epsilon = 1e-06
very_negative = -1e30

VM = pl.BlockSpec(memory_space=pltpu.VMEM)
MESH = pl.DeviceIdType.MESH


def greet(axis, devices):
    barrier = pltpu.get_barrier_semaphore()
    for device in devices:
        pl.semaphore_signal(barrier, inc=1, device_id={axis: device}, device_id_type=MESH)
    pl.semaphore_wait(barrier, len(devices))


def rcopy(src, dst, send, recv, axis, device):
    return pltpu.make_async_remote_copy(
        src_ref=src, dst_ref=dst, send_sem=send, recv_sem=recv,
        device_id={axis: device}, device_id_type=MESH,
    )


def scatter_kernel(n, chunks, a_ref, b_ref, aux_ref, oa_ref, ob_ref, oaux_ref,
                   r1a, r1b, s2a, s2b, r2a, r2b, s1s, s1r, s2s, s2r, axs, axr):
    nx = n // 2
    me = lax.axis_index("dp")
    core = me % 2
    x = me // 2
    partner = me + 1 - 2 * core
    greet("dp", [(me + off) % n for off in range(1, n)])
    started = []
    aux_copies = []
    first = {}
    for g in range(nx):
        xo = (x + 1 + g) % nx
        for c in range(chunks):
            pair = []
            for k, (src, dst) in enumerate(((a_ref, r1a), (b_ref, r1b))):
                cp = rcopy(src.at[xo, 1 - core, c], dst.at[g, c],
                           s1s.at[g, c, k], s1r.at[g, c, k], "dp", partner)
                cp.start()
                pair.append(cp)
                started.append(cp)
            first[g, c] = pair
        if g == 0:
            for off in range(1, n):
                to = (me + off) % n
                cp = rcopy(aux_ref.at[to], oaux_ref.at[me], axs.at[off - 1], axr.at[off - 1], "dp", to)
                cp.start()
                aux_copies.append(cp)
                started.append(cp)
            oaux_ref[me] = aux_ref[me]
    second = {}
    for g in range(nx - 1):
        xo = (x + 1 + g) % nx
        for c in range(chunks):
            pair = []
            for k, (src, got, buf, dst) in enumerate(((a_ref, r1a, s2a, r2a), (b_ref, r1b, s2b, r2b))):
                first[g, c][k].wait_recv()
                buf[g, c] = (
                    src[xo, core, c].astype(jnp.float32) + got[g, c].astype(jnp.float32)
                ).astype(jnp.bfloat16)
                cp = rcopy(buf.at[g, c], dst.at[g, c], s2s.at[g, c, k], s2r.at[g, c, k],
                           "dp", 2 * xo + core)
                cp.start()
                pair.append(cp)
                started.append(cp)
            second[g, c] = pair
    for c in range(chunks):
        for k, (src, got, more, out) in enumerate(((a_ref, r1a, r2a, oa_ref), (b_ref, r1b, r2b, ob_ref))):
            first[nx - 1, c][k].wait_recv()
            total = src[x, core, c].astype(jnp.float32) + got[nx - 1, c].astype(jnp.float32)
            for g in range(nx - 1):
                second[g, c][k].wait_recv()
                total = total + more[g, c].astype(jnp.float32)
            out[c] = total
    for cp in aux_copies:
        cp.wait_recv()
    for cp in started:
        cp.wait_send()


def scatter_dp(n, a, b, aux):
    rows, width = a.shape
    nx = n // 2
    own = rows // n
    chunks = 4 if own % 64 == 0 else 1
    piece = own // chunks
    a = a.reshape(nx, 2, chunks, piece, width)
    b = b.reshape(nx, 2, chunks, piece, width)
    far = max(nx - 1, 1)
    bf = jnp.bfloat16
    sem = pltpu.SemaphoreType.DMA
    oa, ob, oaux = pl.pallas_call(
        functools.partial(scatter_kernel, n, chunks),
        out_shape=(
            jax.ShapeDtypeStruct((chunks, piece, width), jnp.float32),
            jax.ShapeDtypeStruct((chunks, piece, width), jnp.float32),
            jax.ShapeDtypeStruct(aux.shape, jnp.float32),
        ),
        in_specs=[VM] * 3,
        out_specs=(VM,) * 3,
        scratch_shapes=[
            pltpu.VMEM((nx, chunks, piece, width), bf),
            pltpu.VMEM((nx, chunks, piece, width), bf),
            pltpu.VMEM((far, chunks, piece, width), bf),
            pltpu.VMEM((far, chunks, piece, width), bf),
            pltpu.VMEM((far, chunks, piece, width), bf),
            pltpu.VMEM((far, chunks, piece, width), bf),
            sem((nx, chunks, 2)), sem((nx, chunks, 2)),
            sem((far, chunks, 2)), sem((far, chunks, 2)),
            sem((n - 1,)), sem((n - 1,)),
        ],
        compiler_params=pltpu.CompilerParams(collective_id=0, has_side_effects=True),
        name="scatter_dp",
    )(a, b, aux)
    return oa.reshape(own, width), ob.reshape(own, width), oaux


def gather_kernel(n, chunks, m_ref, out_ref, xs, xr, ps, pr, fs, fr):
    nx = n // 2
    me = lax.axis_index("dp")
    core = me % 2
    x = me // 2
    partner = me + 1 - 2 * core
    greet("dp", [partner] + [2 * ((x + 1 + g) % nx) + core for g in range(nx - 1)])
    started = []
    across = {}
    near = {}
    for c in range(chunks):
        for g in range(nx - 1):
            to = 2 * ((x + 1 + g) % nx) + core
            cp = rcopy(m_ref.at[c], out_ref.at[x, core, c], xs.at[g, c], xr.at[g, c], "dp", to)
            cp.start()
            across[g, c] = cp
            started.append(cp)
    for c in range(chunks):
        cp = rcopy(m_ref.at[c], out_ref.at[x, core, c], ps.at[c], pr.at[c], "dp", partner)
        cp.start()
        near[c] = cp
        started.append(cp)
    out_ref[x, core] = m_ref[...]
    passed = []
    for c in range(chunks):
        for g in range(nx - 1):
            origin = (x + nx - 1 - g) % nx
            across[g, c].wait_recv()
            cp = rcopy(out_ref.at[origin, core, c], out_ref.at[origin, core, c],
                       fs.at[g, c], fr.at[g, c], "dp", partner)
            cp.start()
            passed.append(cp)
            started.append(cp)
    for c in range(chunks):
        near[c].wait_recv()
    for cp in passed:
        cp.wait_recv()
    for cp in started:
        cp.wait_send()


def gather_dp(n, m):
    own, width = m.shape
    nx = n // 2
    chunks = 4 if own % 64 == 0 else 1
    piece = own // chunks
    far = max(nx - 1, 1)
    sem = pltpu.SemaphoreType.DMA
    out = pl.pallas_call(
        functools.partial(gather_kernel, n, chunks),
        out_shape=jax.ShapeDtypeStruct((nx, 2, chunks, piece, width), m.dtype),
        in_specs=[VM],
        out_specs=VM,
        scratch_shapes=[
            sem((far, chunks)), sem((far, chunks)), sem((chunks,)), sem((chunks,)),
            sem((far, chunks)), sem((far, chunks)),
        ],
        compiler_params=pltpu.CompilerParams(collective_id=1, has_side_effects=True),
        name="gather_dp",
    )(m.reshape(chunks, piece, width))
    return out.reshape(n * own, width)


def reduce_kernel(n, p_ref, x_ref, out_ref, got, mine, s1, r1, s2, r2):
    me = lax.axis_index("tp")
    greet("tp", [(me + off) % n for off in range(1, n)])
    started = []
    first = []
    order = sorted(range(1, n), key=lambda off: -min(off, n - off))
    for off in order:
        to = (me + off) % n
        cp = rcopy(p_ref.at[to], got.at[off - 1], s1.at[off - 1], r1.at[off - 1], "tp", to)
        cp.start()
        started.append(cp)
        first.append((off, cp))
    total = p_ref[me].astype(jnp.float32)
    for off, cp in first:
        cp.wait_recv()
        total = total + got[off - 1].astype(jnp.float32)
    update = total.astype(jnp.bfloat16).astype(jnp.float32)
    mine[...] = (x_ref[me].astype(jnp.float32) + update).astype(jnp.bfloat16)
    second = []
    for off in order:
        to = (me + off) % n
        cp = rcopy(mine, out_ref.at[me], s2.at[off - 1], r2.at[off - 1], "tp", to)
        cp.start()
        started.append(cp)
        second.append(cp)
    out_ref[me] = mine[...]
    for cp in second:
        cp.wait_recv()
    for cp in started:
        cp.wait_send()


def reduce_tp(n, p, x):
    rows, width = p.shape
    share = rows // n
    sem = pltpu.SemaphoreType.DMA
    out = pl.pallas_call(
        functools.partial(reduce_kernel, n),
        out_shape=jax.ShapeDtypeStruct((n, share, width), jnp.bfloat16),
        in_specs=[VM] * 2,
        out_specs=VM,
        scratch_shapes=[
            pltpu.VMEM((n - 1, share, width), jnp.bfloat16),
            pltpu.VMEM((share, width), jnp.bfloat16),
            sem((n - 1,)), sem((n - 1,)), sem((n - 1,)), sem((n - 1,)),
        ],
        compiler_params=pltpu.CompilerParams(collective_id=2, has_side_effects=True),
        name="reduce_tp",
    )(p.reshape(n, share, width), x.reshape(n, share, width))
    return out.reshape(rows, width)


def cell_kernel(heads, q_ref, k_ref, v_ref, w_ref, s_ref, c_ref, *rest):
    num_ref, new_ref = rest[-2:]
    for h in range(heads):
        q = q_ref[0, h]
        k = k_ref[0, h]
        v = v_ref[0, h]
        scal = s_ref[0, h]
        old = c_ref[0, 0, h]
        scores = lax.dot_general(q, k, (((1,), (1,)), ((), ())), preferred_element_type=jnp.float32)
        scores = scores * w_ref[0, h]
        inside = jnp.dot(scores, v, preferred_element_type=jnp.float32)
        carried = jnp.dot(
            q.astype(jnp.bfloat16), old.astype(jnp.bfloat16), preferred_element_type=jnp.float32
        )
        num_ref[0, h] = inside + scal[:, 0:1] * carried
        outer = lax.dot_general(
            k * scal[:, 1:2], v, (((0,), (0,)), ((), ())), preferred_element_type=jnp.float32
        )
        new_ref[0, 0, h] = scal[0:1, 2:3] * old + outer


def memory_cell(layer, q, k, v, weights, scal, memory, previous):
    batch, heads, steps, dim = q.shape
    row = pl.BlockSpec((1, heads, steps, dim), lambda b: (b, 0, 0, 0))
    small = pl.BlockSpec((1, heads, steps, steps), lambda b: (b, 0, 0, 0))
    three = pl.BlockSpec((1, heads, steps, 3), lambda b: (b, 0, 0, 0))
    mat = pl.BlockSpec((1, 1, heads, dim, dim), lambda b: (layer, b, 0, 0, 0))
    args = [q, k, v, weights, scal, memory]
    specs = [row, row, row, small, three, mat]
    aliases = {}
    if previous is not None:
        args.append(previous)
        specs.append(pl.BlockSpec(memory_space=pl.ANY))
        aliases = {6: 1}
    return pl.pallas_call(
        functools.partial(cell_kernel, heads),
        grid=(batch,),
        out_shape=(
            jax.ShapeDtypeStruct(q.shape, jnp.float32),
            jax.ShapeDtypeStruct(memory.shape, jnp.float32),
        ),
        in_specs=specs,
        out_specs=(row, mat),
        input_output_aliases=aliases,
        compiler_params=pltpu.CompilerParams(dimension_semantics=("arbitrary",)),
        name="memory_cell",
    )(*args)


def per_device(tokens, live_counts, norm_gain, w_branch, w_silu_gate, conv_weight, w_query, w_key,
               w_value, w_input_gate, w_forget_gate, bias_input, bias_forget, out_gain, skip_gain,
               w_out, conv_state, memory, max_state):
    f32 = jnp.float32
    bf = jnp.bfloat16
    ndp = lax.axis_size("dp")
    ntp = lax.axis_size("tp")
    all_batch, steps, features = tokens.shape
    batch = live_counts.shape[0]
    width = w_branch.shape[2]
    heads = w_query.shape[1]
    rows = all_batch * steps
    own = batch * steps
    live_rows = all_batch * steps // 2
    lanes = -(-own // 128) * 128
    model = features * ndp
    flat_tokens = tokens.reshape(rows, features)
    positions = jnp.arange(steps, dtype=jnp.int32)
    live = positions[None, :] < live_counts[:, None]
    causal = positions[:, None] >= positions[None, :]
    picks = live_counts[:, None] + jnp.arange(CONV - 1, dtype=jnp.int32)[None, :]
    pick_hot = picks[:, :, None] == jnp.arange(steps + CONV - 1, dtype=jnp.int32)[None, None, :]
    count_row = jnp.pad(live_counts.astype(f32), (0, lanes - batch))

    dense = flat_tokens
    compact = None
    select = None
    live_all = None
    new_memory = None
    conv_list = []
    max_list = []
    for l in range(LAYERS):
        floats = dense.astype(f32)
        squares = jnp.sum(floats * floats, axis=-1).reshape(ndp, own)
        squares = jnp.pad(squares, ((0, 0), (0, lanes - own)))
        aux = jnp.stack([squares, jnp.broadcast_to(count_row, squares.shape)], axis=1)
        aux = jnp.pad(aux, ((0, 0), (0, 6), (0, 0)))
        scaled = (floats * norm_gain[l]).astype(bf)
        first = jnp.dot(scaled, w_branch[l], preferred_element_type=f32).astype(bf)
        second = jnp.dot(scaled, w_silu_gate[l], preferred_element_type=f32).astype(bf)
        branch, gate, aux = scatter_dp(ndp, first, second, aux)
        total = jnp.sum(aux[:, 0, :own], axis=0)
        inv = lax.rsqrt(total / model + epsilon)[:, None]
        branch = (branch * inv).astype(bf).reshape(batch, steps, width)
        gate = (gate * inv).astype(bf).astype(f32).reshape(batch, steps, width)
        if select is None:
            counts = aux[:, 1, :batch].astype(jnp.int32).reshape(all_batch)
            ids = jnp.arange(all_batch)
            before = jnp.sum(jnp.where(ids[None, :] < ids[:, None], counts[None, :], 0), axis=1)
            live_all = positions[None, :] < counts[:, None]
            place = jnp.where(live_all, before[:, None] + positions[None, :], -1).reshape(rows)
            select = (jnp.arange(live_rows)[:, None] == place[None, :]).astype(bf)
            compact = jnp.dot(select, flat_tokens, preferred_element_type=f32).astype(bf)

        padded = jnp.concatenate([conv_state[l], branch], axis=1).astype(f32)
        conv_sum = padded[:, 0:steps] * conv_weight[l, 0]
        for j in range(1, CONV):
            conv_sum = conv_sum + padded[:, j:j + steps] * conv_weight[l, j]
        convolved = jax.nn.silu(conv_sum).astype(bf)
        new_conv = jnp.stack(
            [jnp.sum(jnp.where(pick_hot[:, i, :, None], padded, 0.0), axis=1) for i in range(CONV - 1)],
            axis=1,
        ).astype(bf)
        conv_list.append(new_conv)
        conv_flat = convolved.reshape(own, width)
        branch_flat = branch.reshape(own, width)

        def project(source, w):
            parts = [
                jnp.dot(source[:, h * HEAD_DIM:(h + 1) * HEAD_DIM], w[h], preferred_element_type=f32)
                for h in range(heads)
            ]
            out = jnp.stack([p.reshape(batch, steps, HEAD_DIM) for p in parts], axis=1)
            return out.astype(bf).astype(f32)

        q = project(conv_flat, w_query[l])
        k = project(conv_flat, w_key[l])
        v = project(branch_flat, w_value[l])

        def gate_dot(w, bias):
            w = w.astype(f32).reshape(heads, 3, 1, HEAD_DIM)
            return jnp.sum(q * w[:, 0] + k * w[:, 1] + v * w[:, 2], axis=-1) + bias[:, None]

        live_h = live[:, None, :]
        ig = jnp.where(live_h, gate_dot(w_input_gate[l], bias_input[l]), very_negative)
        fg = jnp.where(live_h, jax.nn.log_sigmoid(gate_dot(w_forget_gate[l], bias_forget[l])), 0.0)
        cum = jnp.sum(jnp.where(causal, fg[..., None, :], 0.0), axis=-1)
        logw = cum[..., :, None] - cum[..., None, :] + ig[..., None, :]
        logw = jnp.where(causal, logw, very_negative)
        carried = cum + max_state[l][..., None]
        stab = jnp.maximum(jnp.max(logw, axis=-1), carried)
        weights = jnp.exp(logw - stab[..., None])
        new_max = stab[..., -1]
        decay = jnp.exp(cum[..., -1] + max_state[l] - new_max)
        upd = jnp.exp(cum[..., -1:] - cum + ig - new_max[..., None])
        scal = jnp.stack(
            [jnp.exp(carried - stab), upd, jnp.broadcast_to(decay[..., None], upd.shape)], axis=-1
        )
        max_list.append(new_max)
        num, new_memory = memory_cell(
            l, q, k * HEAD_DIM ** (-0.5), v, weights, scal, memory, new_memory
        )
        centered = num - jnp.mean(num, axis=-1, keepdims=True)
        normalized = centered * lax.rsqrt(
            jnp.mean(centered * centered, axis=-1, keepdims=True) + epsilon
        )
        normalized = normalized * out_gain[l][None, :, None, :]
        readout = jnp.transpose(normalized, (0, 2, 1, 3)).reshape(batch, steps, width)
        mixed = (readout + skip_gain[l] * convolved.astype(f32)) * jax.nn.silu(gate)
        mixed = jnp.where(live[:, :, None], mixed, 0.0).astype(bf).reshape(own, width)
        everyone = gather_dp(ndp, mixed)
        packed = jnp.dot(select, everyone, preferred_element_type=f32).astype(bf)
        part = jnp.dot(packed, w_out[l], preferred_element_type=f32).astype(bf)
        compact = reduce_tp(ntp, part, compact)
        dense = lax.dot_general(
            select, compact, (((0,), (0,)), ((), ())), preferred_element_type=f32
        ).astype(bf)
    result = jnp.where(live_all[:, :, None], dense.reshape(tokens.shape), tokens)
    return (result, jnp.stack(conv_list), new_memory, jnp.stack(max_list))


def solution(mesh):
    in_specs = (
        P("grp", None, "dp"),
        P(("grp", "dp")),
        P(None, "dp"),
        P(None, "dp", "tp"),
        P(None, "dp", "tp"),
        P(None, None, "tp"),
        P(None, "tp", None, None),
        P(None, "tp", None, None),
        P(None, "tp", None, None),
        P(None, "tp", None),
        P(None, "tp", None),
        P(None, "tp"),
        P(None, "tp"),
        P(None, "tp", None),
        P(None, "tp"),
        P(None, "tp", "dp"),
        P(None, ("grp", "dp"), None, "tp"),
        P(None, ("grp", "dp"), "tp", None, None),
        P(None, ("grp", "dp"), "tp"),
    )
    out_specs = (
        P("grp", None, "dp"),
        P(None, ("grp", "dp"), None, "tp"),
        P(None, ("grp", "dp"), "tp", None, None),
        P(None, ("grp", "dp"), "tp"),
    )
    return jax.shard_map(
        per_device, mesh=mesh, in_specs=in_specs, out_specs=out_specs, check_vma=False
    )
```

time: 298 us -> 203 us (0.68)
  Pallas kernels: 0 us -> 139 us
  waiting for transfers between devices: 93 us -> 0 us
  blocking collectives: 54.3 us -> 0 us
  matrix products: 65.3 us -> 24.4 us
  local copies, waits for them, and re-layouts: 27.7 us -> 7.49 us
  between operations: 15 us -> 1.35 us
  other arithmetic: 41.4 us -> 28.6 us
    pallas_call x0 -> x8, Pallas kernels: none -> 139 us  [the longest x2 42.8 us: memory_cell(): pl.pallas_call(functools.partial(cell_kernel, heads), grid=(batch,), out_...]
    unnamed x8 -> x0, waiting for transfers between devices: 54.4 us -> none
    dot_general x22 -> x33, matrix products: 65.3 us -> 24.4 us  [the longest x2 5.92 us: per_device(): part = jnp.dot(packed, w_out[l], preferred_element_type=f32).astype(bf)]
    all_gather x2 -> x0, blocking collectives: 31.1 us -> none  [layer_step(): lax.all_gather(new_share, 'tp', axis=0, tiled=True)]
    another operation x8 -> x6, other arithmetic: 30.1 us -> 1.33 us  [the longest x2 1.3 us: per_device(): return (result, jnp.stack(conv_list), new_memory, jnp.stack(max_list))]
    psum x2 -> x0, blocking collectives: 23.2 us -> none  [layer_step(): total_squares = lax.psum(partial_squares, 'dp')]
    reduce_scatter x2 -> x0, waiting for transfers between devices: 21.8 us -> none  [layer_step(): lax.psum_scatter(flat_terms.astype(jnp.bfloat16), 'tp', scatter_dimension...]
    all_gather x2 -> x0, waiting for transfers between devices: 16.8 us -> none  [layer_step(): piece = lax.all_gather(mixed, 'dp', axis=0, tiled=True)]
  transfers between devices with their start and end apart: 6 -> 0, of which waited for: 4 -> 0; matrix products, arithmetic and copies ran while one was open for 17% -> 0% of each run, Pallas kernels for 0% -> 0%
where the time goes in v1:
time: 203 us; the launch traced here: 201 us
  Pallas kernels  139 us (68%)
  other arithmetic  28.6 us (14%)
  matrix products  24.4 us (12%)
  local copies, waits for them, and re-layouts  7.49 us (4%)
    pallas_call x2, Pallas kernels, memory_cell(): pl.pallas_call(functools.partial(cell_kernel, heads), grid=(batch,), out_...  42.8 us
    pallas_call x2, Pallas kernels, scatter_dp(): pl.pallas_call(functools.partial(scatter_kernel, n, chunks), out_shape=(j...  37.9 us
    pallas_call x2, Pallas kernels, reduce_tp(): pl.pallas_call(functools.partial(reduce_kernel, n), out_shape=jax.ShapeDt...  35.4 us
    pallas_call x2, Pallas kernels, gather_dp(): pl.pallas_call(functools.partial(gather_kernel, n, chunks), out_shape=jax...  23.2 us
    dot_general x2, matrix products, per_device(): part = jnp.dot(packed, w_out[l], preferred_element_type=f32).astype(bf)  5.92 us
    dot_general x2, matrix products, per_device(): first = jnp.dot(scaled, w_branch[l], preferred_element_type=f32).astype(bf)  4.91 us
    dot_general x2, matrix products, per_device(): jnp.dot(scaled, w_silu_gate[l], preferred_element_type=f32).astype(bf)  4.81 us
    dot_general x24, matrix products, project(): jnp.dot(source[:, h * HEAD_DIM:(h + 1) * HEAD_DIM], w[h], preferred_eleme...  4.12 us

profile of v1, /device:TPU:0, one launch (start us, length us, event | category | flops | bytes accessed | tf_op | source)
XLA Modules:
  0.0 201.1 jit_solution(12372474992132130793)
XLA Ops:
  1.5 3.1 %convolution_convert_fusion.3 = bf16[512,1024]{1,0:T(8,128)(2,1)} fusion(bf16[2,512,1024]{2,1,0:T(8,128)(2,1)} %param.22, bf16[64,8,512]{2,1,0:T(8,128)(2,1)} %param.19, f32[512]{0:T(512)S(1)} %bitcast.491), kind=kOutput, calls=%fused_computation.3 | convolution fusion | flops 538181632 | bytes 2623488 | tf_op jit(solution)/shard_map/dot_general | solution.py:333
  4.6 1.7 convolution_convert_fusion.2
  7.2 19.5 %scatter_dp.2 = (f32[4,32,1024]{2,1,0:T(8,128)}, f32[4,32,1024]{2,1,0:T(8,128)}, f32[4,8,128]{2,1,0:T(8,128)}) custom-call(bf16[2,2,4,32,1024]{4,3,2,1,0:T(8,128)(2,1)} %bitcast.443, bf16[2,2,4,32,1024]{4,3,2,1,0:T(8,128)(2,1)} %bitcast.444, f32[4,8,128]{2,1,0:T(8,128)} %pad.12.aux_ref), custom_call_target="tpu_custom_call" | custom-call | tf_op jit(solution)/shard_map/scatter_dp/pallas_call | solution.py:105
  27.5 1.1 multiply_convert_fusion.5
  32.6 1.0 fusion.58
  35.3 1.0 copy.141.s_ref
  37.2 1.0 maximum_convert_fusion
  38.3 21.5 %memory_cell.2 = (f32[16,4,8,256]{3,2,1,0:T(8,128)}, f32[2,16,4,256,256]{4,3,2,1,0:T(8,128)}) custom-call(f32[16,4,8,256]{3,2,1,0:T(8,128)} %get-tuple-element.90.q_ref, f32[16,4,8,256]{3,2,1,0:T(8,128)} %get-tuple-element.36.k_ref, f32[16,4,8,256]{3,2,1,0:T(8,128)} %get-tuple-element.91.v_ref, f32[16,4,8,8]{3,2,1,0:T(8,128)} %subtract_exponential_fusion.1.w_ref, ...), custom_call_target="tpu_custom_call" | custom-call | tf_op jit(solution)/shard_map/memory_cell/pallas_call | solution.py:280
  59.8 1.3 reduce_sum.205
  61.1 1.3 multiply_reduce_fusion.1
  62.4 1.2 multiply_multiply_fusion.1
  63.7 1.2 fusion.79
  65.0 12.1 %gather_dp.2 = bf16[2,2,4,32,1024]{4,3,2,1,0:T(8,128)(2,1)} custom-call(bf16[4,32,1024]{2,1,0:T(8,128)(2,1)} %bitcast.440), custom_call_target="tpu_custom_call" | custom-call | tf_op jit(solution)/shard_map/gather_dp/pallas_call | solution.py:179
  78.2 3.0 %fusion.4 = bf16[256,512]{1,0:T(8,128)(2,1)} fusion(bf16[512,1024]{1,0:T(8,128)(2,1)} %bitcast.441, bf16[2,1024,512]{2,1,0:T(8,128)(2,1)} %param.34, s32[512]{0:T(512)S(1)} %select_n.124), kind=kOutput, calls=%fused_computation.16 | convolution fusion | flops 537395200 | bytes 2361344 | tf_op jit(solution)/shard_map/dot_general | solution.py:407
  81.2 1.0 convolution_convert_fusion.8
  82.2 18.4 %reduce_tp.2.x_ref = bf16[4,64,512]{2,1,0:T(8,128)(2,1)} custom-call(bf16[4,64,512]{2,1,0:T(8,128)(2,1)} %bitcast.450, bf16[4,64,512]{2,1,0:T(8,128)(2,1)} %bitcast.452), custom_call_target="tpu_custom_call" | custom-call | tf_op jit(solution)/shard_map/reduce_tp/pallas_call | solution.py:230
  100.6 1.5 fusion.33
  102.1 3.1 %convolution_convert_fusion = bf16[512,1024]{1,0:T(8,128)(2,1)} fusion(bf16[2,512,1024]{2,1,0:T(8,128)(2,1)} %param.23, bf16[512,512]{0,1:T(8,128)(2,1)S(1)} %get-tuple-element.87, f32[512]{0:T(512)S(1)} %bitcast.488), kind=kOutput, calls=%fused_computation | convolution fusion | flops 538181632 | bytes 2623488 | tf_op jit(solution)/shard_map/dot_general | solution.py:334
  105.2 1.8 convolution_convert_fusion.1
  107.7 18.5 %scatter_dp.3 = (f32[4,32,1024]{2,1,0:T(8,128)}, f32[4,32,1024]{2,1,0:T(8,128)}, f32[4,8,128]{2,1,0:T(8,128)}) custom-call(bf16[2,2,4,32,1024]{4,3,2,1,0:T(8,128)(2,1)} %bitcast.446, bf16[2,2,4,32,1024]{4,3,2,1,0:T(8,128)(2,1)} %bitcast.445, f32[4,8,128]{2,1,0:T(8,128)} %pad.13.aux_ref), custom_call_target="tpu_custom_call" | custom-call | tf_op jit(solution)/shard_map/scatter_dp/pallas_call | solution.py:105
  127.0 1.1 multiply_convert_fusion.2
  128.4 2.1 %select_reduce_fusion.2 = (bf16[16,1024]{1,0:T(8,128)(2,1)S(1)}, bf16[16,1024]{1,0:T(8,128)(2,1)S(1)}, bf16[16,1024]{1,0:T(8,128)(2,1)S(1)}, bf16[16,1024]{1,0:T...) fusion(pred[16,11]{1,0:T(8,128)(4,1)S(1)} %get-tuple-element.73, ...), kind=kLoop, calls=%fused_computation.79 | loop fusion | flops 3506176 | bytes 918032 | tf_op jit(solution)/shard_map/reduce_sum | solution.py:355
  137.3 1.0 copy.149.s_ref
  140.9 21.3 %memory_cell.3 = (f32[16,4,8,256]{3,2,1,0:T(8,128)}, f32[2,16,4,256,256]{4,3,2,1,0:T(8,128)}) custom-call(f32[16,4,8,256]{3,2,1,0:T(8,128)} %maximum_convert_fusion.2.q_ref, f32[16,4,8,256]{3,2,1,0:T(8,128)} %get-tuple-element.34.k_ref, f32[16,4,8,256]{3,2,1,0:T(8,128)} %maximum_convert_fusion.3.v_ref, ...), custom_call_target="tpu_custom_call", output_to_operand_aliasing={{1}: (6, {})} | custom-call | tf_op jit(solution)/shard_map/memory_cell/pallas_call | solution.py:280
  162.2 1.2 reduce_sum.214
  163.5 1.3 multiply_reduce_fusion
  164.8 1.2 multiply_multiply_fusion
  166.1 1.2 fusion.78
  167.3 11.1 %gather_dp.3 = bf16[2,2,4,32,1024]{4,3,2,1,0:T(8,128)(2,1)} custom-call(bf16[4,32,1024]{2,1,0:T(8,128)(2,1)} %bitcast.439), custom_call_target="tpu_custom_call" | custom-call | tf_op jit(solution)/shard_map/gather_dp/pallas_call | solution.py:179
  178.4 3.0 %fusion.3 = bf16[256,512]{1,0:T(8,128)(2,1)} fusion(bf16[512,1024]{1,0:T(8,128)(2,1)} %bitcast.442, bf16[2,1024,512]{2,1,0:T(8,128)(2,1)} %param.34, s32[512]{0:T(512)S(1)} %select_n.124), kind=kOutput, calls=%fused_computation.15 | convolution fusion | flops 537395200 | bytes 2361344 | tf_op jit(solution)/shard_map/dot_general | solution.py:407
  181.4 17.0 %reduce_tp.3 = bf16[4,64,512]{2,1,0:T(8,128)(2,1)} custom-call(bf16[4,64,512]{2,1,0:T(8,128)(2,1)} %bitcast.451, bf16[4,64,512]{2,1,0:T(8,128)(2,1)} %reduce_tp.2.x_ref), custom_call_target="tpu_custom_call" | custom-call | tf_op jit(solution)/shard_map/reduce_tp/pallas_call | solution.py:230
  198.4 2.1 %fusion.29 = bf16[64,8,512]{2,1,0:T(8,128)(2,1)} fusion(bf16[64,8,512]{2,1,0:T(8,128)(2,1)S(1)} %copy-done.8, bf16[256,512]{1,0:T(8,128)(2,1)} %bitcast.449, pred[64,8]{1,0:T(8,128)(4,1)S(1)} %iota_compare_fusion.9, s32[512]{0:T(512)S(1)} %select_n.124), kind=kOutput, calls=%fused_computation.66 | convolution fusion | flops 134873088 | bytes 1313280 | tf_op jit(solution)/shard_map/dot_general | solution.py:409
  (167 shorter events, 21.6 us)
Async XLA Ops:
  0.6 4.0 %copy-start.7 = (bf16[64,8,512]{2,1,0:T(8,128)(2,1)S(1)}, bf16[64,8,512]{2,1,0:T(8,128)(2,1)}, u32[]{:S(2)}) copy-start(bf16[64,8,512]{2,1,0:T(8,128)(2,1)} %param.19) | copy-start | bytes 1572868
  0.6 4.0 %copy-start.21 = (bf16[2,512,1024]{2,1,0:T(8,128)(2,1)S(1)}, bf16[2,512,1024]{2,1,0:T(8,128)(2,1)}, u32[]{:S(2)}) copy-start(bf16[2,512,1024]{2,1,0:T(8,128)(2,1)} %param.23) | copy-start | bytes 6291460
  4.6 1.7 copy-start.18
  6.3 22.4 %copy-start.11 = (bf16[2,16,3,1024]{3,1,2,0:T(8,128)(2,1)S(1)}, bf16[2,16,3,1024]{3,1,2,0:T(8,128)(2,1)}, u32[]{:S(2)}) copy-start(bf16[2,16,3,1024]{3,1,2,0:T(8,128)(2,1)} %param.35) | copy-start | bytes 589828
  7.2 21.8 %copy-start.12 = (f32[2,4,1024]{2,1,0:T(4,128)S(1)}, f32[2,4,1024]{2,1,0:T(4,128)}, u32[]{:S(2)}) copy-start(f32[2,4,1024]{2,1,0:T(4,128)} %param.24) | copy-start | bytes 98308
  28.7 1.2 copy-start.3
  29.0 1.6 copy-start.5
  29.1 2.3 %copy-start.1 = (f32[4,32,1024]{2,1,0:T(8,128)S(1)}, f32[4,32,1024]{2,1,0:T(8,128)}, u32[]{:S(2)}) copy-start(f32[4,32,1024]{2,1,0:T(8,128)} %get-tuple-element.15) | copy-start | bytes 1572868
  29.1 2.4 %copy-start.2 = (bf16[2,4,256,256]{3,2,1,0:T(8,128)(2,1)S(1)}, bf16[2,4,256,256]{3,2,1,0:T(8,128)(2,1)}, u32[]{:S(2)}) copy-start(bf16[2,4,256,256]{3,2,1,0:T(8,128)(2,1)} %param.27) | copy-start | bytes 3145732
  30.0 2.3 %copy-start.14 = (bf16[2,4,768]{2,1,0:T(4,128)(2,1)S(1)}, bf16[2,4,768]{2,1,0:T(4,128)(2,1)}, u32[]{:S(2)}) copy-start(bf16[2,4,768]{2,1,0:T(4,128)(2,1)} %param.28) | copy-start | bytes 36868
  30.3 2.2 %copy-start.15 = (bf16[2,4,768]{2,1,0:T(4,128)(2,1)S(1)}, bf16[2,4,768]{2,1,0:T(4,128)(2,1)}, u32[]{:S(2)}) copy-start(bf16[2,4,768]{2,1,0:T(4,128)(2,1)} %param.29) | copy-start | bytes 36868
  31.4 2.2 %copy-start.19 = (f32[2,4]{1,0:T(2,128)S(1)}, f32[2,4]{1,0:T(2,128)}, u32[]{:S(2)}) copy-start(f32[2,4]{1,0:T(2,128)} %param.30) | copy-start | bytes 100
  31.4 2.2 %copy-start.20 = (f32[2,4]{1,0:T(2,128)S(1)}, f32[2,4]{1,0:T(2,128)}, u32[]{:S(2)}) copy-start(f32[2,4]{1,0:T(2,128)} %param.31) | copy-start | bytes 100
  31.4 2.9 %copy-start.13 = (f32[2,16,4]{1,2,0:T(4,128)S(1)}, f32[2,16,4]{1,2,0:T(4,128)}, u32[]{:S(2)}) copy-start(f32[2,16,4]{1,2,0:T(4,128)} %param.37) | copy-start | bytes 1540
  38.3 24.1 %copy-start.16 = (f32[2,4,256]{2,1,0:T(4,128)S(1)}, f32[2,4,256]{2,1,0:T(4,128)}, u32[]{:S(2)}) copy-start(f32[2,4,256]{2,1,0:T(4,128)} %param.32) | copy-start | bytes 24580
  59.8 3.9 %copy-start.17 = (f32[2,1024]{1,0:T(2,128)S(1)}, f32[2,1024]{1,0:T(2,128)}, u32[]{:S(2)}) copy-start(f32[2,1024]{1,0:T(2,128)} %param.33) | copy-start | bytes 24580
  59.8 3.9 %copy-start.10 = (f32[4,32,1024]{2,1,0:T(8,128)S(1)}, f32[4,32,1024]{2,1,0:T(8,128)}, u32[]{:S(2)}) copy-start(f32[4,32,1024]{2,1,0:T(8,128)} %get-tuple-element.17) | copy-start | bytes 1572868
  64.9 16.2 %copy-start.8 = (bf16[64,8,512]{2,1,0:T(8,128)(2,1)S(1)}, bf16[64,8,512]{2,1,0:T(8,128)(2,1)}, u32[]{:S(2)}) copy-start(bf16[64,8,512]{2,1,0:T(8,128)(2,1)} %param.19) | copy-start | bytes 1572868
  100.6 4.6 %copy-start.22 = (bf16[2,512,1024]{2,1,0:T(8,128)(2,1)S(1)}, bf16[2,512,1024]{2,1,0:T(8,128)(2,1)}, u32[]{:S(2)}) copy-start(bf16[2,512,1024]{2,1,0:T(8,128)(2,1)} %param.22) | copy-start | bytes 6291460
  126.1 5.1 %copy-start = (f32[4,32,1024]{2,1,0:T(8,128)S(1)}, f32[4,32,1024]{2,1,0:T(8,128)}, u32[]{:S(2)}) copy-start(f32[4,32,1024]{2,1,0:T(8,128)} %get-tuple-element.18) | copy-start | bytes 1572868
  131.9 1.2 copy-start.4
  132.0 1.7 copy-start.6
  162.2 3.9 %copy-start.9 = (f32[4,32,1024]{2,1,0:T(8,128)S(1)}, f32[4,32,1024]{2,1,0:T(8,128)}, u32[]{:S(2)}) copy-start(f32[4,32,1024]{2,1,0:T(8,128)} %get-tuple-element.22) | copy-start | bytes 1572868

commit v2 on v1

--- a/solution.py
+++ b/solution.py
@@ -243,43 +243,55 @@
     return out.reshape(rows, width)
 
 
-def cell_kernel(heads, q_ref, k_ref, v_ref, w_ref, s_ref, c_ref, *rest):
+def cell_kernel(per, heads, low, q_ref, k_ref, v_ref, w_ref, s_ref, g_ref, c_ref, *rest):
     num_ref, new_ref = rest[-2:]
-    for h in range(heads):
-        q = q_ref[0, h]
-        k = k_ref[0, h]
-        v = v_ref[0, h]
-        scal = s_ref[0, h]
-        old = c_ref[0, 0, h]
-        scores = lax.dot_general(q, k, (((1,), (1,)), ((), ())), preferred_element_type=jnp.float32)
-        scores = scores * w_ref[0, h]
-        inside = jnp.dot(scores, v, preferred_element_type=jnp.float32)
-        carried = jnp.dot(
-            q.astype(jnp.bfloat16), old.astype(jnp.bfloat16), preferred_element_type=jnp.float32
-        )
-        num_ref[0, h] = inside + scal[:, 0:1] * carried
-        outer = lax.dot_general(
-            k * scal[:, 1:2], v, (((0,), (0,)), ((), ())), preferred_element_type=jnp.float32
-        )
-        new_ref[0, 0, h] = scal[0:1, 2:3] * old + outer
-
-
-def memory_cell(layer, q, k, v, weights, scal, memory, previous):
+    narrow = jnp.bfloat16 if low else jnp.float32
+    for i in range(per):
+        for h in range(heads):
+            q = q_ref[i, h]
+            k = k_ref[i, h]
+            v = v_ref[i, h]
+            scal = s_ref[i, h]
+            old = c_ref[0, i, h]
+            outer = lax.dot_general(
+                (k * scal[:, 1:2]).astype(narrow), v.astype(narrow), (((0,), (0,)), ((), ())),
+                preferred_element_type=jnp.float32,
+            )
+            new_ref[0, i, h] = scal[0:1, 2:3] * old + outer
+            carried = jnp.dot(
+                q.astype(jnp.bfloat16), old.astype(jnp.bfloat16), preferred_element_type=jnp.float32
+            )
+            scores = lax.dot_general(
+                q.astype(narrow), k.astype(narrow), (((1,), (1,)), ((), ())),
+                preferred_element_type=jnp.float32,
+            )
+            scores = scores * w_ref[i, h]
+            inside = jnp.dot(
+                scores.astype(narrow), v.astype(narrow), preferred_element_type=jnp.float32
+            )
+            num = inside + scal[:, 0:1] * carried
+            centered = num - jnp.mean(num, axis=-1, keepdims=True)
+            spread = jnp.mean(centered * centered, axis=-1, keepdims=True)
+            num_ref[i, h] = centered * lax.rsqrt(spread + epsilon) * g_ref[h:h + 1, :]
+
+
+def memory_cell(layer, q, k, v, weights, scal, gain, memory, previous, per=4, low=True):
     batch, heads, steps, dim = q.shape
-    row = pl.BlockSpec((1, heads, steps, dim), lambda b: (b, 0, 0, 0))
-    small = pl.BlockSpec((1, heads, steps, steps), lambda b: (b, 0, 0, 0))
-    three = pl.BlockSpec((1, heads, steps, 3), lambda b: (b, 0, 0, 0))
-    mat = pl.BlockSpec((1, 1, heads, dim, dim), lambda b: (layer, b, 0, 0, 0))
-    args = [q, k, v, weights, scal, memory]
-    specs = [row, row, row, small, three, mat]
+    per = per if batch % per == 0 else 1
+    row = pl.BlockSpec((per, heads, steps, dim), lambda b: (b, 0, 0, 0))
+    small = pl.BlockSpec((per, heads, steps, steps), lambda b: (b, 0, 0, 0))
+    three = pl.BlockSpec((per, heads, steps, 3), lambda b: (b, 0, 0, 0))
+    mat = pl.BlockSpec((1, per, heads, dim, dim), lambda b: (layer, b, 0, 0, 0))
+    args = [q, k, v, weights, scal, gain, memory]
+    specs = [row, row, row, small, three, pl.BlockSpec((heads, dim), lambda b: (0, 0)), mat]
     aliases = {}
     if previous is not None:
         args.append(previous)
         specs.append(pl.BlockSpec(memory_space=pl.ANY))
-        aliases = {6: 1}
+        aliases = {7: 1}
     return pl.pallas_call(
-        functools.partial(cell_kernel, heads),
-        grid=(batch,),
+        functools.partial(cell_kernel, per, heads, low),
+        grid=(batch // per,),
         out_shape=(
             jax.ShapeDtypeStruct(q.shape, jnp.float32),
             jax.ShapeDtypeStruct(memory.shape, jnp.float32),
@@ -329,7 +341,7 @@
         squares = jnp.pad(squares, ((0, 0), (0, lanes - own)))
         aux = jnp.stack([squares, jnp.broadcast_to(count_row, squares.shape)], axis=1)
         aux = jnp.pad(aux, ((0, 0), (0, 6), (0, 0)))
-        scaled = (floats * norm_gain[l]).astype(bf)
+        scaled = lax.optimization_barrier((floats * norm_gain[l]).astype(bf))
         first = jnp.dot(scaled, w_branch[l], preferred_element_type=f32).astype(bf)
         second = jnp.dot(scaled, w_silu_gate[l], preferred_element_type=f32).astype(bf)
         branch, gate, aux = scatter_dp(ndp, first, second, aux)
@@ -344,6 +356,7 @@
             live_all = positions[None, :] < counts[:, None]
             place = jnp.where(live_all, before[:, None] + positions[None, :], -1).reshape(rows)
             select = (jnp.arange(live_rows)[:, None] == place[None, :]).astype(bf)
+            select = lax.optimization_barrier(select)
             compact = jnp.dot(select, flat_tokens, preferred_element_type=f32).astype(bf)
 
         padded = jnp.concatenate([conv_state[l], branch], axis=1).astype(f32)
@@ -391,14 +404,9 @@
             [jnp.exp(carried - stab), upd, jnp.broadcast_to(decay[..., None], upd.shape)], axis=-1
         )
         max_list.append(new_max)
-        num, new_memory = memory_cell(
-            l, q, k * HEAD_DIM ** (-0.5), v, weights, scal, memory, new_memory
+        normalized, new_memory = memory_cell(
+            l, q, k * HEAD_DIM ** (-0.5), v, weights, scal, out_gain[l], memory, new_memory
         )
-        centered = num - jnp.mean(num, axis=-1, keepdims=True)
-        normalized = centered * lax.rsqrt(
-            jnp.mean(centered * centered, axis=-1, keepdims=True) + epsilon
-        )
-        normalized = normalized * out_gain[l][None, :, None, :]
         readout = jnp.transpose(normalized, (0, 2, 1, 3)).reshape(batch, steps, width)
         mixed = (readout + skip_gain[l] * convolved.astype(f32)) * jax.nn.silu(gate)
         mixed = jnp.where(live[:, :, None], mixed, 0.0).astype(bf).reshape(own, width)

time: 203 us -> 209 us (1.030)
  local copies, waits for them, and re-layouts: 7.49 us -> 23.2 us
  Pallas kernels: 139 us -> 130 us
    pallas_call x2, Pallas kernels: 42.8 us -> 33.1 us  [memory_cell(): pl.pallas_call(functools.partial(cell_kernel, per, heads, low), grid=(bat...]
    reduce_sum x4 -> x0, other arithmetic: 5.12 us -> none  [the longest x2 2.62 us: per_device(): jnp.mean(centered * centered, axis=-1, keepdims=True) + epsilon]
    mul x2 -> x0, other arithmetic: 2.49 us -> none  [per_device(): normalized = normalized * out_gain[l][None, :, None, :]]
    convert_element_type x2, other arithmetic: 2.43 us -> 4.67 us  [per_device(): jnp.where(live[:, :, None], mixed, 0.0).astype(bf).reshape(own, width)]
where the time goes in v2:
time: 209 us; the launch traced here: 207 us
  Pallas kernels  130 us (62%)
  other arithmetic  29.3 us (14%)
  matrix products  23.8 us (11%)
  local copies, waits for them, and re-layouts  23.2 us (11%)
    pallas_call x2, Pallas kernels, scatter_dp(): pl.pallas_call(functools.partial(scatter_kernel, n, chunks), out_shape=(j...  37.9 us
    pallas_call x2, Pallas kernels, reduce_tp(): pl.pallas_call(functools.partial(reduce_kernel, n), out_shape=jax.ShapeDt...  35.4 us
    pallas_call x2, Pallas kernels, memory_cell(): pl.pallas_call(functools.partial(cell_kernel, per, heads, low), grid=(bat...  33.1 us
    pallas_call x2, Pallas kernels, gather_dp(): pl.pallas_call(functools.partial(gather_kernel, n, chunks), out_shape=jax...  23.1 us
    dot_general x2, matrix products, per_device(): part = jnp.dot(packed, w_out[l], preferred_element_type=f32).astype(bf)  5.92 us
    dot_general x2, matrix products, per_device(): first = jnp.dot(scaled, w_branch[l], preferred_element_type=f32).astype(bf)  5.86 us
    convert_element_type x2, other arithmetic, per_device(): jnp.where(live[:, :, None], mixed, 0.0).astype(bf).reshape(own, width)  4.67 us

profile of v2, /device:TPU:0, one launch (start us, length us, event | category | flops | bytes accessed | tf_op | source)
XLA Modules:
  0.0 207.3 jit_solution(8760561351226602990)
XLA Ops:
  0.6 1.4 fusion.148
  2.1 1.1 multiply_convert_fusion
  3.2 2.9 %convolution_convert_fusion.3 = bf16[512,1024]{1,0:T(8,128)(2,1)} fusion(bf16[512,512]{1,0:T(8,128)(2,1)S(1)} %multiply_convert_fusion, bf16[2,512,1024]{2,1,0:T(8,128)(2,1)} %param.22), kind=kOutput, calls=%fused_computation.3 | convolution fusion | flops 537395200 | bytes 2621440 | tf_op jit(solution)/shard_map/dot_general | solution.py:345
  6.1 1.7 convolution_convert_fusion.2
  8.8 19.4 %scatter_dp.2 = (f32[4,32,1024]{2,1,0:T(8,128)}, f32[4,32,1024]{2,1,0:T(8,128)}, f32[4,8,128]{2,1,0:T(8,128)}) custom-call(bf16[2,2,4,32,1024]{4,3,2,1,0:T(8,128)(2,1)} %bitcast.447, bf16[2,2,4,32,1024]{4,3,2,1,0:T(8,128)(2,1)} %bitcast.448, f32[4,8,128]{2,1,0:T(8,128)} %pad.12.aux_ref), custom_call_target="tpu_custom_call" | custom-call | tf_op jit(solution)/shard_map/scatter_dp/pallas_call | solution.py:105
  29.0 1.1 multiply_convert_fusion.6
  43.1 1.4 copy.140
  44.6 1.4 copy.136
  46.7 1.4 copy.137
  48.8 1.4 copy.139
  53.1 1.8 copy.141.s_ref
  54.9 1.7 subtract_exponential_fusion.1.w_ref
  56.6 1.9 maximum_convert_fusion
  58.5 1.3 slice_bitcast_fusion.57
  59.9 16.5 %memory_cell.2 = (f32[16,4,8,256]{3,2,1,0:T(8,128)}, f32[2,16,4,256,256]{4,3,2,1,0:T(8,128)}) custom-call(f32[16,4,8,256]{3,2,1,0:T(8,128)} %get-tuple-element.90.q_ref, f32[16,4,8,256]{3,2,1,0:T(8,128)} %get-tuple-element.38.k_ref, f32[16,4,8,256]{3,2,1,0:T(8,128)} %get-tuple-element.91.v_ref, f32[16,4,8,8]{3,2,1,0:T(8,128)} %subtract_exponential_fusion.1.w_ref, ...), custom_call_target="tpu_custom_call" | custom-call | tf_op jit(solution)/shard_map/memory_cell/pallas_call | solution.py:292
  76.5 2.4 %fusion.76 = bf16[16,8,1024]{2,1,0:T(8,128)(2,1)} fusion(f32[16,8,1024]{2,1,0:T(8,128)} %bitcast.455, f32[16,8,1024]{2,1,0:T(8,128)} %bitcast.453, f32[1024]{0:T(1024)S(1)} %bitcast.492, f32[16,8]{1,0:T(8,128)S(1)} %rsqrt.23, pred[16,8]{1,0:T(8,128)(4,1)S(1)} %iota_compare_fusion.4, f32[1024]{0:T(1024)S(1)} %bitcast.474, f32[16,11,1024]{2,1,0:T(8,128)S(1)} %fusion.81, ...), kind=kLoop, calls=%fused_computation.148 | loop fusion | flops 3276800 | bytes 3428992 | tf_op jit(solution)/shard_map/convert_element_type | solution.py:412
  78.9 12.1 %gather_dp.2 = bf16[2,2,4,32,1024]{4,3,2,1,0:T(8,128)(2,1)} custom-call(bf16[4,32,1024]{2,1,0:T(8,128)(2,1)} %bitcast.444), custom_call_target="tpu_custom_call" | custom-call | tf_op jit(solution)/shard_map/gather_dp/pallas_call | solution.py:179
  92.1 3.0 %fusion.4 = bf16[256,512]{1,0:T(8,128)(2,1)} fusion(bf16[256,512]{1,0:T(8,128)(2,1)S(1)} %fusion.77, bf16[512,1024]{1,0:T(8,128)(2,1)} %bitcast.445, bf16[2,1024,512]{2,1,0:T(8,128)(2,1)} %param.34), kind=kOutput, calls=%fused_computation.14 | convolution fusion | flops 537264128 | bytes 2621440 | tf_op jit(solution)/shard_map/dot_general | solution.py:415
  96.1 18.4 %reduce_tp.2.x_ref = bf16[4,64,512]{2,1,0:T(8,128)(2,1)} custom-call(bf16[4,64,512]{2,1,0:T(8,128)(2,1)} %bitcast.457, bf16[4,64,512]{2,1,0:T(8,128)(2,1)} %bitcast.451), custom_call_target="tpu_custom_call" | custom-call | tf_op jit(solution)/shard_map/reduce_tp/pallas_call | solution.py:230
  114.5 1.5 fusion.31
  116.0 2.9 %convolution_convert_fusion.1 = bf16[512,1024]{1,0:T(8,128)(2,1)} fusion(bf16[512,512]{0,1:T(8,128)(2,1)S(1)} %get-tuple-element.34, bf16[2,512,1024]{2,1,0:T(8,128)(2,1)} %param.22), kind=kOutput, calls=%fused_computation.1 | convolution fusion | flops 537395200 | bytes 2621440 | tf_op jit(solution)/shard_map/dot_general | solution.py:345
  119.0 1.7 convolution_convert_fusion
  121.3 18.4 %scatter_dp.3 = (f32[4,32,1024]{2,1,0:T(8,128)}, f32[4,32,1024]{2,1,0:T(8,128)}, f32[4,8,128]{2,1,0:T(8,128)}) custom-call(bf16[2,2,4,32,1024]{4,3,2,1,0:T(8,128)(2,1)} %bitcast.449, bf16[2,2,4,32,1024]{4,3,2,1,0:T(8,128)(2,1)} %bitcast.450, f32[4,8,128]{2,1,0:T(8,128)} %pad.13.aux_ref), custom_call_target="tpu_custom_call" | custom-call | tf_op jit(solution)/shard_map/scatter_dp/pallas_call | solution.py:105
  140.7 1.1 multiply_convert_fusion.3
  142.0 2.1 %select_reduce_fusion.2 = (bf16[16,1024]{1,0:T(8,128)(2,1)S(1)}, bf16[16,1024]{1,0:T(8,128)(2,1)S(1)}, bf16[16,1024]{1,0:T(8,128)(2,1)S(1)}, bf16[16,1024]{1,0:T...) fusion(pred[16,11]{1,0:T(8,128)(4,1)S(1)} %get-tuple-element.75, ...), kind=kLoop, calls=%fused_computation.75 | loop fusion | flops 3506176 | bytes 918032 | tf_op jit(solution)/shard_map/reduce_sum | solution.py:368
  151.0 1.1 copy.149.s_ref
  154.7 16.6 %memory_cell.3 = (f32[16,4,8,256]{3,2,1,0:T(8,128)}, f32[2,16,4,256,256]{4,3,2,1,0:T(8,128)}) custom-call(f32[16,4,8,256]{3,2,1,0:T(8,128)} %maximum_convert_fusion.2.q_ref, f32[16,4,8,256]{3,2,1,0:T(8,128)} %get-tuple-element.36.k_ref, f32[16,4,8,256]{3,2,1,0:T(8,128)} %maximum_convert_fusion.3.v_ref, ...), custom_call_target="tpu_custom_call", output_to_operand_aliasing={{1}: (7, {})} | custom-call | tf_op jit(solution)/shard_map/memory_cell/pallas_call | solution.py:292
  171.3 2.3 %fusion.75 = bf16[16,8,1024]{2,1,0:T(8,128)(2,1)} fusion(f32[16,8,1024]{2,1,0:T(8,128)} %bitcast.454, f32[16,8,1024]{2,1,0:T(8,128)S(1)} %bitcast.452, f32[1024]{0:T(1024)S(1)} %bitcast.491, f32[16,8]{1,0:T(8,128)S(1)} %rsqrt.25, pred[16,8]{1,0:T(8,128)(4,1)S(1)} %iota_compare_fusion.4, f32[1024]{0:T(1024)S(1)} %bitcast.470, ...), kind=kLoop, calls=%fused_computation.147 | loop fusion | flops 3276800 | bytes 3428992 | tf_op jit(solution)/shard_map/convert_element_type | solution.py:412
  173.5 11.1 %gather_dp.3 = bf16[2,2,4,32,1024]{4,3,2,1,0:T(8,128)(2,1)} custom-call(bf16[4,32,1024]{2,1,0:T(8,128)(2,1)} %bitcast.443), custom_call_target="tpu_custom_call" | custom-call | tf_op jit(solution)/shard_map/gather_dp/pallas_call | solution.py:179
  184.6 3.0 %fusion.3 = bf16[256,512]{1,0:T(8,128)(2,1)} fusion(bf16[256,512]{1,0:T(8,128)(2,1)S(1)} %fusion.77, bf16[512,1024]{1,0:T(8,128)(2,1)} %bitcast.446, bf16[2,1024,512]{2,1,0:T(8,128)(2,1)} %param.34), kind=kOutput, calls=%fused_computation.13 | convolution fusion | flops 537264128 | bytes 2621440 | tf_op jit(solution)/shard_map/dot_general | solution.py:415
  187.6 17.0 %reduce_tp.3 = bf16[4,64,512]{2,1,0:T(8,128)(2,1)} custom-call(bf16[4,64,512]{2,1,0:T(8,128)(2,1)} %bitcast.458, bf16[4,64,512]{2,1,0:T(8,128)(2,1)} %reduce_tp.2.x_ref), custom_call_target="tpu_custom_call" | custom-call | tf_op jit(solution)/shard_map/reduce_tp/pallas_call | solution.py:230
  204.6 2.1 %fusion.29 = bf16[64,8,512]{2,1,0:T(8,128)(2,1)} fusion(bf16[64,8,512]{2,1,0:T(8,128)(2,1)S(1)} %copy-done, bf16[256,512]{1,0:T(8,128)(2,1)S(1)} %fusion.77, bf16[256,512]{1,0:T(8,128)(2,1)} %bitcast.456, pred[64,8]{1,0:T(8,128)(4,1)S(1)} %iota_compare_fusion.2), kind=kOutput, calls=%fused_computation.64 | convolution fusion | flops 134742016 | bytes 1573376 | tf_op jit(solution)/shard_map/dot_general | solution.py:417
  (213 shorter events, 32.4 us)
Async XLA Ops:
  0.6 5.5 %copy-start.48 = (bf16[2,512,1024]{2,1,0:T(8,128)(2,1)S(1)}, bf16[2,512,1024]{2,1,0:T(8,128)(2,1)}, u32[]{:S(2)}) copy-start(bf16[2,512,1024]{2,1,0:T(8,128)(2,1)} %param.23) | copy-start | bytes 6291460
  7.8 22.4 %copy-start.13 = (bf16[2,16,3,1024]{3,1,2,0:T(8,128)(2,1)S(1)}, bf16[2,16,3,1024]{3,1,2,0:T(8,128)(2,1)}, u32[]{:S(2)}) copy-start(bf16[2,16,3,1024]{3,1,2,0:T(8,128)(2,1)} %param.35) | copy-start | bytes 589828
  7.9 23.3 %copy-start.32 = (f32[4,1,128]{2,1,0:T(1,128)}, f32[4,1,128]{2,1,0:T(1,128)S(1)}, u32[]{:S(2)}) copy-start(f32[4,1,128]{2,1,0:T(1,128)S(1)} %stack_broadcast_in_dim.6) | copy-start | bytes 6148
  8.8 22.4 %copy-start.26 = (f32[2,4,1024]{2,1,0:T(4,128)S(1)}, f32[2,4,1024]{2,1,0:T(4,128)}, u32[]{:S(2)}) copy-start(f32[2,4,1024]{2,1,0:T(4,128)} %param.24) | copy-start | bytes 98308
  31.1 2.3 %copy-start.6 = (bf16[2,4,256,256]{3,2,1,0:T(8,128)(2,1)S(1)}, bf16[2,4,256,256]{3,2,1,0:T(8,128)(2,1)}, u32[]{:S(2)}) copy-start(bf16[2,4,256,256]{3,2,1,0:T(8,128)(2,1)} %param.26) | copy-start | bytes 3145732
  32.7 2.3 %copy-start.36 = (bf16[2,4,768]{2,1,0:T(4,128)(2,1)S(1)}, bf16[2,4,768]{2,1,0:T(4,128)(2,1)}, u32[]{:S(2)}) copy-start(bf16[2,4,768]{2,1,0:T(4,128)(2,1)} %param.28) | copy-start | bytes 36868
  33.1 2.8 %copy-start.37 = (bf16[2,4,768]{2,1,0:T(4,128)(2,1)S(1)}, bf16[2,4,768]{2,1,0:T(4,128)(2,1)}, u32[]{:S(2)}) copy-start(bf16[2,4,768]{2,1,0:T(4,128)(2,1)} %param.29) | copy-start | bytes 36868
  34.2 3.3 %copy-start.46 = (f32[2,4]{1,0:T(2,128)S(1)}, f32[2,4]{1,0:T(2,128)}, u32[]{:S(2)}) copy-start(f32[2,4]{1,0:T(2,128)} %param.30) | copy-start | bytes 100
  34.2 3.3 %copy-start.47 = (f32[2,4]{1,0:T(2,128)S(1)}, f32[2,4]{1,0:T(2,128)}, u32[]{:S(2)}) copy-start(f32[2,4]{1,0:T(2,128)} %param.31) | copy-start | bytes 100
  34.2 5.6 %copy-start.34 = (f32[2,16,4]{1,2,0:T(4,128)S(1)}, f32[2,16,4]{1,2,0:T(4,128)}, u32[]{:S(2)}) copy-start(f32[2,16,4]{1,2,0:T(4,128)} %param.37) | copy-start | bytes 1540
  35.0 3.2 %copy-start.8 = (bf16[16,1,8,256]{3,2,1,0:T(8,128)(2,1)}, bf16[16,1,8,256]{3,2,1,0:T(8,128)(2,1)S(1)}, u32[]{:S(2)}) copy-start(bf16[16,1,8,256]{3,2,1,0:T(8,128)(2,1)S(1)} %fusion.16) | copy-start | bytes 196612
  35.9 2.4 %copy-start.11 = (f32[16,4,8]{2,1,0:T(4,128)}, f32[16,4,8]{2,1,0:T(4,128)S(1)}, u32[]{:S(2)}) copy-start(f32[16,4,8]{2,1,0:T(4,128)S(1)} %fusion.59) | copy-start | bytes 6148
  38.0 2.3 %copy-start.41 = (f32[4]{0:T(128)}, f32[4]{0:T(128)S(1)}, u32[]{:S(2)}) copy-start(f32[4]{0:T(128)S(1)} %get-tuple-element.87) | copy-start | bytes 52
  59.8 16.6 %copy-start.39 = (f32[2,1024]{1,0:T(2,128)S(1)}, f32[2,1024]{1,0:T(2,128)}, u32[]{:S(2)}) copy-start(f32[2,1024]{1,0:T(2,128)} %param.33) | copy-start | bytes 24580
  59.8 16.6 %copy-start.19 = (f32[1,1,1024]{2,1,0:T(1,128)S(1)}, f32[1,1,1024]{2,1,0:T(1,128)}, u32[]{:S(2)}) copy-start(f32[1,1,1024]{2,1,0:T(1,128)} %copy-done.18) | copy-start | bytes 12292
  59.8 16.6 %copy-start.21 = (f32[1,1,1024]{2,1,0:T(1,128)S(1)}, f32[1,1,1024]{2,1,0:T(1,128)}, u32[]{:S(2)}) copy-start(f32[1,1,1024]{2,1,0:T(1,128)} %copy-done.20) | copy-start | bytes 12292
  59.8 16.6 %copy-start.23 = (f32[1,1,1024]{2,1,0:T(1,128)S(1)}, f32[1,1,1024]{2,1,0:T(1,128)}, u32[]{:S(2)}) copy-start(f32[1,1,1024]{2,1,0:T(1,128)} %copy-done.22) | copy-start | bytes 12292
  59.8 16.6 %copy-start.25 = (f32[1,1,1024]{2,1,0:T(1,128)S(1)}, f32[1,1,1024]{2,1,0:T(1,128)}, u32[]{:S(2)}) copy-start(f32[1,1,1024]{2,1,0:T(1,128)} %copy-done.24) | copy-start | bytes 12292
  92.1 22.4 %copy-start.45 = (f32[1,512]{1,0:T(1,128)S(1)}, f32[1,512]{1,0:T(1,128)}, u32[]{:S(2)}) copy-start(f32[1,512]{1,0:T(1,128)} %get-tuple-element.78) | copy-start | bytes 6148
  114.5 4.4 %copy-start.49 = (bf16[2,512,1024]{2,1,0:T(8,128)(2,1)S(1)}, bf16[2,512,1024]{2,1,0:T(8,128)(2,1)}, u32[]{:S(2)}) copy-start(bf16[2,512,1024]{2,1,0:T(8,128)(2,1)} %param.23) | copy-start | bytes 6291460
  120.7 21.1 %copy-start.10 = (bf16[16,3,1024]{2,0,1:T(8,128)(2,1)S(1)}, bf16[16,3,1024]{2,0,1:T(8,128)(2,1)}, u32[]{:S(2)}) copy-start(bf16[16,3,1024]{2,0,1:T(8,128)(2,1)} %get-tuple-element.39) | copy-start | bytes 294916
  120.7 21.2 %copy-start.44 = (s32[16]{0:T(128)S(1)}, s32[16]{0:T(128)}, u32[]{:S(2)}) copy-start(s32[16]{0:T(128)} %param.20) | copy-start | bytes 196
  139.8 5.2 %copy-start.1 = (f32[4,32,1024]{2,1,0:T(8,128)S(1)}, f32[4,32,1024]{2,1,0:T(8,128)}, u32[]{:S(2)}) copy-start(f32[4,32,1024]{2,1,0:T(8,128)} %get-tuple-element.18) | copy-start | bytes 1572868
  145.9 2.3 %copy-start.28 = (bf16[1,4,768]{2,1,0:T(4,128)(2,1)S(1)}, bf16[1,4,768]{2,1,0:T(4,128)(2,1)}, u32[]{:S(2)}) copy-start(bf16[1,4,768]{2,1,0:T(4,128)(2,1)} %get-tuple-element.61) | copy-start | bytes 18436
  145.9 2.5 %copy-start.29 = (bf16[1,4,768]{2,1,0:T(4,128)(2,1)S(1)}, bf16[1,4,768]{2,1,0:T(4,128)(2,1)}, u32[]{:S(2)}) copy-start(bf16[1,4,768]{2,1,0:T(4,128)(2,1)} %get-tuple-element.56) | copy-start | bytes 18436
  146.9 2.5 %copy-start.40 = (f32[4]{0:T(128)S(1)}, f32[4]{0:T(128)}, u32[]{:S(2)}) copy-start(f32[4]{0:T(128)} %get-tuple-element.86) | copy-start | bytes 52
  146.9 2.5 %copy-start.42 = (f32[4]{0:T(128)S(1)}, f32[4]{0:T(128)}, u32[]{:S(2)}) copy-start(f32[4]{0:T(128)} %get-tuple-element.89) | copy-start | bytes 52
  147.1 3.0 %copy-start.30 = (f32[16,4]{0,1:T(4,128)S(1)}, f32[16,4]{0,1:T(4,128)}, u32[]{:S(2)}) copy-start(f32[16,4]{0,1:T(4,128)} %get-tuple-element.76) | copy-start | bytes 772
  147.5 3.4 %copy-start.38 = (pred[16,8]{0,1:T(8,128)(4,1)S(1)}, pred[16,8]{0,1:T(8,128)(4,1)}, u32[]{:S(2)}) copy-start(pred[16,8]{0,1:T(8,128)(4,1)} %copy.138) | copy-start | bytes 388
  147.5 3.5 %copy-start.35 = (f32[2,16,4]{1,2,0:T(4,128)S(1)}, f32[2,16,4]{1,2,0:T(4,128)}, u32[]{:S(2)}) copy-start(f32[2,16,4]{1,2,0:T(4,128)} %param.37) | copy-start | bytes 1540
  154.7 16.6 %copy-start.9 = (f32[4,32,1024]{2,1,0:T(8,128)S(1)}, f32[4,32,1024]{2,1,0:T(8,128)}, u32[]{:S(2)}) copy-start(f32[4,32,1024]{2,1,0:T(8,128)} %get-tuple-element.22) | copy-start | bytes 1572868
  187.6 19.1 %copy-start.27 = (f32[16,4,1]{0,1,2:T(4,128)S(1)}, f32[16,4,1]{0,1,2:T(4,128)}, u32[]{:S(2)}) copy-start(f32[16,4,1]{0,1,2:T(4,128)} %copy.140) | copy-start | bytes 772
  (18 other events, 24.2 us)
